TPU v7x, 32 devices: a whole 2x2x4 slice. The times are simulated.
32 devices in a mesh: ep: 8 (over z, core), tp: 4 (over y, x).
Axes of the slice: x: 2, y: 2, z: 4, core: 2. Of those that a mesh axis runs over, the one named last changes fastest.
Arguments:
- queries: bfloat16 [1024, 1536], P('ep', 'tp'), may hold values from -64 to 64
- kv_latent: bfloat16 [1024, 512], P('ep'), may hold values from -60 to 60
- rope_key: bfloat16 [1024, 32], P('ep'), may hold values from -64 to 64
- latent_gain: float32 [512], replicated, may hold values from 0.1 to 1.9
- key_up: bfloat16 [512, 1024], P(None, 'tp'), may hold values from -0.25 to 0.25
- value_up: bfloat16 [512, 1024], P(None, 'tp'), may hold values from -40 to 40
- query_gain: float32 [96], replicated, may hold values from 0.3 to 4
- key_gain: float32 [96], replicated, may hold values from 0.3 to 4
- out_gain: float32 [1024], replicated, may hold values from 0.1 to 1.9
- out_proj: bfloat16 [1024, 4096], P(None, 'tp'), may hold values from -0.1875 to 0.1875
- moe_input: bfloat16 [1024, 4096], P('ep'), may hold values from -60 to 60
- moe_gain: float32 [4096], replicated, may hold values from 0.1 to 1.9
- expert_ids: int32 [1024, 2], P('ep'), may hold values from 0 to 31, as said below
- route_weights: float32 [1024, 2], P('ep'), may hold values from 0.2 to 1
- w_gate: bfloat16 [32, 4096, 2048], P('ep', None, 'tp'), may hold values from -0.09375 to 0.09375
- w_up: bfloat16 [32, 4096, 2048], P('ep', None, 'tp'), may hold values from -0.09375 to 0.09375
- w_down: bfloat16 [32, 2048, 4096], P('ep', 'tp'), may hold values from -0.125 to 0.125
Outputs:
- mixed: bfloat16 [1024, 4096], P('ep', 'tp')
- expert_out: bfloat16 [1024, 4096], P('ep', 'tp')
Inputs may be any that keep to these rules, and one draw needn't show every extreme that they name: `expert_ids`: both experts of a row lie in one group (g * 8 to g * 8 + 7) and differ. In each aligned block of 128 rows no expert is named more than 12 times, and some expert is named exactly 12 times.
All inputs are finite; a program needn't handle non-finite values.
Results may differ from a plain program's by a relative error of at most 0.015.
The roundings to bfloat16 on the way count: a program that leaves them out, or rounds other values in their place, can miss the bound.
Values may be sent and summed in bfloat16 or wider, within the bound.
No kernel may reach another device: no remote copies, remote signals or barrier semaphores. Data moves between devices by JAX's collectives and lax.ppermute only.
A program may use at most 128 MiB of HBM per device.

v0:
```python
import jax
import jax.numpy as jnp
from jax import lax
from jax.sharding import PartitionSpec as P

NOPE = 64
ROPE = 32
VDIM = 64
QKD = 96
CAP = 12


EPS = 1e-06
THETA = 10000.0


def rotate_half(values_in, positions):
    half_width = ROPE // 2
    inverse = THETA ** (-jnp.arange(half_width, dtype=jnp.float32) / half_width)
    angles = positions.astype(jnp.float32)[:, None] * inverse
    cosine = jnp.cos(angles)[:, None, :]
    sine = jnp.sin(angles)[:, None, :]
    first_half = values_in[..., :half_width]
    second_half = values_in[..., half_width:]
    return jnp.concatenate(
        [first_half * cosine - second_half * sine, second_half * cosine + first_half * sine],
        axis=-1,
    )


def head_norm(values_in, gain_vec):
    return (
        values_in
        * lax.rsqrt(jnp.mean(values_in * values_in, axis=-1, keepdims=True) + EPS)
        * gain_vec
    )


def make_queries(queries, query_gain, positions):
    row_count = queries.shape[0]
    head_count = queries.shape[1] // QKD
    normed = head_norm(queries.astype(jnp.float32).reshape(row_count, head_count, QKD), query_gain)
    turned = jnp.concatenate(
        [normed[..., :NOPE], rotate_half(normed[..., NOPE:], positions)], axis=-1
    )
    return turned.astype(jnp.bfloat16)


def make_keys(latent, rope_part, latent_gain, key_up, value_up, key_gain, positions):
    row_count = latent.shape[0]
    head_count = key_up.shape[1] // NOPE
    latent_f = latent.astype(jnp.float32)
    latent_n = (
        latent_f
        * lax.rsqrt(jnp.mean(latent_f * latent_f, axis=-1, keepdims=True) + EPS)
        * latent_gain
    ).astype(jnp.bfloat16)
    key_nope = jnp.dot(latent_n, key_up, preferred_element_type=jnp.float32).astype(jnp.bfloat16)
    key_nope = lax.optimization_barrier(key_nope)
    value_rows = jnp.dot(latent_n, value_up, preferred_element_type=jnp.float32).astype(
        jnp.bfloat16
    )
    shared = jnp.broadcast_to(
        rope_part.astype(jnp.float32)[:, None, :], (row_count, head_count, ROPE)
    )
    key_full = jnp.concatenate(
        [key_nope.astype(jnp.float32).reshape(row_count, head_count, NOPE), shared], axis=-1
    )
    normed = head_norm(key_full, key_gain)
    turned = jnp.concatenate(
        [normed[..., :NOPE], rotate_half(normed[..., NOPE:], positions)], axis=-1
    )
    return (turned.astype(jnp.bfloat16), value_rows.reshape(row_count, head_count, VDIM))


def shards(
    queries,
    kv_latent,
    rope_key,
    latent_gain,
    key_up,
    value_up,
    query_gain,
    key_gain,
    out_gain,
    out_proj,
    moe_input,
    moe_gain,
    expert_ids,
    route_weights,
    w_gate,
    w_up,
    w_down,
):
    tok_rows = queries.shape[0]
    head_count = key_up.shape[1] // NOPE
    query_pos = lax.axis_index("ep") * tok_rows + jnp.arange(tok_rows, dtype=jnp.int32)
    query_rot = make_queries(queries, query_gain, query_pos)
    inv_scale = QKD ** (-0.5)
    blocks_in = (
        lax.all_gather(kv_latent, "ep", axis=0, tiled=True),
        lax.all_gather(rope_key, "ep", axis=0, tiled=True),
    )
    key_pos = jnp.arange(blocks_in[0].shape[0], dtype=jnp.int32)
    key_rot, value_rows = make_keys(
        blocks_in[0], blocks_in[1], latent_gain, key_up, value_up, key_gain, key_pos
    )
    top_prev = jnp.full((head_count, tok_rows), -1e30, jnp.float32)
    key_pos = jnp.arange(key_rot.shape[0], dtype=jnp.int32)
    scores = (
        jnp.einsum("qhd,khd->hqk", query_rot, key_rot, preferred_element_type=jnp.float32)
        * inv_scale
    )
    visible = key_pos[None, :] <= query_pos[:, None]
    scores = jnp.where(visible[None], scores, -1e30)
    top_new = jnp.maximum(top_prev, jnp.max(scores, axis=-1))
    expo = jnp.exp(scores - top_new[..., None])
    total_new = jnp.sum(expo, axis=-1)
    accum_new = jnp.einsum(
        "hqk,khd->hqd", expo.astype(jnp.bfloat16), value_rows, preferred_element_type=jnp.float32
    )
    attn = (accum_new / total_new[..., None]).astype(jnp.bfloat16)
    attn = attn.transpose(1, 0, 2).reshape(tok_rows, head_count * VDIM)
    block_f = lax.all_gather(attn, "tp", axis=1, tiled=True).astype(jnp.float32)
    scaled = (block_f * out_gain[None, :]).astype(jnp.bfloat16)
    product = jnp.dot(scaled, out_proj, preferred_element_type=jnp.float32)
    product, squares = (product, jnp.sum(block_f * block_f, axis=-1))
    mixed = (product * lax.rsqrt(squares / out_gain.shape[0] + EPS)[:, None]).astype(jnp.bfloat16)
    row_count = moe_input.shape[0]
    top_count = expert_ids.shape[1]
    local_experts = w_gate.shape[0]
    ep_count = lax.axis_size("ep")
    expert_count = local_experts * ep_count
    stream_f = moe_input.astype(jnp.float32)
    normed = (
        stream_f * lax.rsqrt(jnp.mean(stream_f * stream_f, axis=-1, keepdims=True) + EPS) * moe_gain
    ).astype(jnp.bfloat16)
    flat_ids = expert_ids.reshape(-1)
    onehot = (flat_ids[:, None] == jnp.arange(expert_count, dtype=jnp.int32)[None, :]).astype(
        jnp.int32
    )
    slot_rank = jnp.sum((jnp.cumsum(onehot, axis=0) - onehot) * onehot, axis=1)
    slot_index = flat_ids * CAP + slot_rank
    token_index = jnp.arange(row_count * top_count, dtype=jnp.int32) // top_count
    slot_token = jnp.zeros((expert_count * CAP,), jnp.int32).at[slot_index].set(token_index)
    slot_used = jnp.zeros((expert_count * CAP,), jnp.bool_).at[slot_index].set(True)
    outgoing = jnp.where(slot_used[:, None], normed[slot_token], jnp.zeros((), jnp.bfloat16))
    outgoing = outgoing.reshape(ep_count, local_experts, CAP, normed.shape[1])
    piece_width = normed.shape[1] // lax.axis_size("tp")
    my_columns = lax.dynamic_slice_in_dim(
        outgoing, lax.axis_index("tp") * piece_width, piece_width, 3
    )
    arrived_part = lax.all_to_all(my_columns, "ep", split_axis=0, concat_axis=0, tiled=True)
    piece = lax.all_gather(arrived_part, "tp", axis=3, tiled=True)
    gate_acc = jnp.einsum("secd,edf->secf", piece, w_gate, preferred_element_type=jnp.float32)
    upper_acc = jnp.einsum("secd,edf->secf", piece, w_up, preferred_element_type=jnp.float32)
    hidden = (jax.nn.silu(gate_acc) * upper_acc).astype(jnp.bfloat16)
    out_cols = w_down.shape[2] // lax.axis_size("tp")
    term = jnp.einsum("secf,efd->dsec", hidden, w_down, preferred_element_type=jnp.float32)
    summed = lax.psum_scatter(
        term.reshape(lax.axis_size("tp") * out_cols, -1).astype(jnp.bfloat16),
        "tp",
        scatter_dimension=0,
        tiled=True,
    )
    expert_y = summed.T.reshape(ep_count, local_experts * CAP, out_cols)
    returned_rows = lax.all_to_all(expert_y, "ep", split_axis=0, concat_axis=0, tiled=True).reshape(
        expert_count * CAP, out_cols
    )
    picked = returned_rows[slot_index].reshape(row_count, top_count, out_cols).astype(jnp.float32)
    expert_out = jnp.sum(picked * route_weights[..., None], axis=1).astype(jnp.bfloat16)
    return (mixed, expert_out)


def solution(mesh):
    in_specs = (
        P("ep", "tp"),
        P("ep", None),
        P("ep", None),
        P(),
        P(None, "tp"),
        P(None, "tp"),
        P(),
        P(),
        P(),
        P(None, "tp"),
        P("ep", None),
        P(),
        P("ep", None),
        P("ep", None),
        P("ep", None, "tp"),
        P("ep", None, "tp"),
        P("ep", "tp", None),
    )
    out_specs = (P("ep", "tp"), P("ep", "tp"))
    return jax.shard_map(shards, mesh=mesh, in_specs=in_specs, out_specs=out_specs, check_vma=False)
```

profile of v0, /device:TPU:0, one launch (start us, length us, event | category | flops | bytes accessed | tf_op | source)
XLA Modules:
  0.0 224.2 jit_solution(16331249084519766166)
XLA Ops:
  7.2 0.9 copy.35
  8.4 0.7 broadcast_multiply_fusion
  9.1 0.6 reduce-window.6
  9.7 0.2 slice_reduce_fusion
  10.3 1.4 scatter_custom_fusion.1
  11.8 1.5 fusion.15
  13.3 1.6 fusion.17
  14.8 4.1 %gather_fusion = bf16[384,4096]{1,0:T(8,128)(2,1)} fusion(bf16[128,4096]{1,0:T(8,128)(2,1)S(1)} %fusion.17, s32[1024]{0:T(1024)S(1)} %pad_clamp_fusion.1), kind=kCustom, calls=%fused_computation | custom fusion | bytes 6292992 | tf_op jit(solution)/shard_map/gather | solution.py:147
  18.9 5.5 %gather.9 = bf16[8,4,12,4096]{3,2,1,0:T(8,128)(2,1)} reshape(bf16[384,4096]{1,0:T(8,128)(2,1)} %gather_fusion) | data formatting | bytes 6291456 | tf_op jit(solution)/shard_map/gather | solution.py:147
  24.4 1.5 scatter_custom_fusion
  26.0 1.5 dynamic-slice_select_fusion
  27.5 0.6 copy.38
  28.1 27.1 %all_to_all.10 = bf16[8,4,12,1024]{3,1,2,0:T(4,128)(2,1)S(1)} all-to-all(bf16[8,4,12,1024]{3,1,2,0:T(4,128)(2,1)S(1)} %copy.38), channel_id=1, replica_groups=mesh['ep'=8,'tp'=4] {'ep'}, dimensions={0} | all-to-all | bytes 1572864 | tf_op jit(solution)/shard_map/all_to_all | solution.py:153
  55.2 1.3 copy.39
  56.5 0.7 all-gather.3.cloned.1.call-update
  57.3 0.2 reduce-scatter.2.cloned.1.call-start
  57.5 50.7 %all-gather.5.cloned.1.call-done = bf16[8,4,12,4096]{3,2,0,1:T(8,128)(2,1)} async-done(((bf16[8,4,12,1024]{3,2,0,1:T(8,128)(2,1)}), bf16[8,4,12,4096]{3,2,0,1:T(8,128)(2,1)}) %all-gather.5.cloned.1.call-update) | async-done | bytes 3145744 | tf_op jit(solution)/shard_map/all_gather | solution.py:154
  108.2 9.5 %fusion.21 = f32[8,4,12,512]{3,2,0,1:T(8,128)S(1)} fusion(bf16[8,4,12,4096]{3,2,0,1:T(8,128)(2,1)} %all-gather.5.cloned.1.call-done, bf16[4,4096,512]{2,1,0:T(8,128)(2,1)} %param.31), kind=kOutput, calls=%fused_computation.30 | convolution fusion | flops 1610612736 | bytes 20709376 | tf_op jit(solution)/shard_map/secd,edf->secf/dot_general | solution.py:155
  117.7 9.7 %fusion.30 = bf16[8,4,12,512]{3,2,0,1:T(8,128)(2,1)S(1)} fusion(bf16[8,4,12,4096]{3,2,0,1:T(8,128)(2,1)} %all-gather.5.cloned.1.call-done, bf16[4,4096,512]{2,1,0:T(8,128)(2,1)} %param.32, f32[8,4,12,512]{3,2,0,1:T(8,128)S(1)} %fusion.21), kind=kOutput, calls=%fused_computation.33 | convolution fusion | flops 1611792384 | bytes 21102592 | tf_op jit(solution)/shard_map/secd,edf->secf/dot_general | solution.py:156
  127.5 4.3 %fusion.9 = bf16[4096,8,4,12]{0,3,1,2:T(8,128)(2,1)} fusion(bf16[8,4,12,512]{3,2,0,1:T(8,128)(2,1)S(1)} %fusion.30, bf16[4,512,4096]{2,1,0:T(8,128)(2,1)S(1)} %bitcast.84), kind=kOutput, calls=%fused_computation.11 | convolution fusion | flops 1612185600 | bytes 20316160 | tf_op jit(solution)/shard_map/secf,efd->dsec/dot_general | solution.py:159
  131.8 4.6 %copy.40 = bf16[4096,8,4,12]{0,3,2,1:T(8,128)(2,1)} copy(bf16[4096,8,4,12]{0,3,1,2:T(8,128)(2,1)} %fusion.9) | data formatting | bytes 6291456 | tf_op jit(solution)/shard_map/convert_element_type | solution.py:161
  136.4 5.6 %convert_element_type.108 = bf16[4096,384]{0,1:T(8,128)(2,1)} reshape(bf16[4096,8,4,12]{0,3,2,1:T(8,128)(2,1)} %copy.40) | data formatting | bytes 6291456 | tf_op jit(solution)/shard_map/convert_element_type | solution.py:161
  142.1 0.8 copy-done.3
  143.2 0.6 slice.63
  144.0 12.8 %all_gather.13 = bf16[1024,32]{0,1:T(8,128)(2,1)S(1)} all-gather(bf16[128,32]{0,1:T(8,128)(2,1)S(1)} %copy-done.6), channel_id=1, replica_groups=mesh['ep'=8,'tp'=4] {'ep'}, dimensions={0}, use_global_device_ids=true | all-gather | bytes 73728 | tf_op jit(solution)/shard_map/all_gather | solution.py:102
  156.7 0.6 pad_clamp_fusion
  157.5 0.6 subtract_convert_fusion.1
  158.2 0.3 multiply_cosine_fusion
  158.6 1.6 fusion.12
  160.2 0.6 copy-done.8
  160.8 2.6 %convolution_convert_fusion.1 = bf16[1024,256]{1,0:T(8,128)(2,1)} fusion(bf16[512,256]{1,0:T(8,128)(2,1)S(1)} %copy-done.13, bf16[1024,512]{1,0:T(8,128)(2,1)} %all-gather.3.cloned.1.call-done, f32[512]{0:T(512)S(1)} %copy-done.15, f32[1024]{0:T(1024)S(1)} %add_rsqrt_fusion.1), kind=kOutput, calls=%fused_computation.35 | convolution fusion | flops 270794752 | bytes 1841152 | tf_op jit(solution)/shard_map/dot_general | solution.py:58
  163.3 1.2 copy.33
  164.6 0.2 multiply_reduce_fusion
  164.8 0.4 copy-done.12
  165.2 0.4 multiply_multiply_fusion
  165.8 0.3 copy-done.4
  166.1 2.0 fusion.18
  168.0 18.2 %reduce-scatter.2.cloned.1.call-done = bf16[1024,384]{0,1:T(8,128)(2,1)} async-done(((bf16[4096,384]{0,1:T(8,128)(2,1)}), bf16[1024,384]{0,1:T(8,128)(2,1)}) %reduce-scatter.2.cloned.1.call-update) | async-done | bytes 786448 | tf_op jit(solution)/shard_map/reduce_scatter | solution.py:160
  186.2 4.6 %all-to-all-start.1 = ((bf16[8,48,1024]{2,1,0:T(8,128)(2,1)}), bf16[8,48,1024]{2,1,0:T(8,128)(2,1)S(1)}, u32[]{:S(2)}, u32[]{:S(2)}) async-start(bf16[8,48,1024]{2,1,0:T(8,128)(2,1)} %bitcast.89), calls=%async_computation.2 | async-start | bytes 1572864 | tf_op jit(solution)/shard_map/all_to_all | solution.py:167
  190.9 2.3 %fusion.19 = f32[4,128]{1,0:T(4,128)S(1)} fusion(f32[4,128,1024]{2,1,0:T(8,128)} %get-tuple-element.11, f32[4,128]{1,0:T(4,128)S(1)} %broadcast_maximum_fusion, pred[128,1024]{1,0:T(8,128)(4,1)S(1)} %iota_compare_fusion), kind=kLoop, calls=%fused_computation.25 | loop fusion | flops 2096640 | bytes 2232320 | tf_op jit(solution)/shard_map/reduce_sum | solution.py:118
  193.2 0.7 convolution_convert_fusion
  193.9 0.7 fusion.35
  194.7 8.9 %all_gather.14 = bf16[128,1024]{0,1:T(8,128)(2,1)S(1)} all-gather(bf16[128,256]{0,1:T(8,128)(2,1)S(1)} %bitcast.90), channel_id=1, replica_groups=mesh['ep'=8,'tp'=4] {'tp'}, dimensions={1}, use_global_device_ids=true | all-gather | bytes 327680 | tf_op jit(solution)/shard_map/all_gather | solution.py:124
  203.8 1.4 fusion.33
  205.2 6.6 %all-to-all-done.1 = bf16[8,48,1024]{2,1,0:T(8,128)(2,1)S(1)} async-done(((bf16[8,48,1024]{2,1,0:T(8,128)(2,1)}), bf16[8,48,1024]{2,1,0:T(8,128)(2,1)S(1)}, u32[]{:S(2)}, u32[]{:S(2)}) %all-to-all-start.1) | async-done | bytes 786464 | tf_op jit(solution)/shard_map/all_to_all | solution.py:167
  211.8 2.1 gather_fusion.1
  213.9 1.7 reshape.278
  215.6 2.1 multiply_reduce_fusion.1
  (78 shorter events, 2.0 us)
Async XLA Ops:
  7.2 196.6 %copy-start = (bf16[1024,1024]{1,0:T(8,128)(2,1)S(1)}, bf16[1024,1024]{1,0:T(8,128)(2,1)}, u32[]{:S(2)}) copy-start(bf16[1024,1024]{1,0:T(8,128)(2,1)} %param.26) | copy-start | bytes 6291460
  7.2 101.0 %all-gather.5.cloned.1.call-start = ((), (), s32[]{:S(2)}) async-start(), calls=%async_computation.4 | async-start | bytes 5242880 | tf_op jit(solution)/shard_map/all_gather | solution.py:154
  56.5 102.1 %all-gather.3.cloned.1.call-start = ((), (), s32[]{:S(2)}) async-start(), calls=%async_computation.3 | async-start | bytes 1179648 | tf_op jit(solution)/shard_map/all_gather | solution.py:101
  57.3 129.0 %reduce-scatter.2.cloned.1.call-start = ((), (), s32[]{:S(2)}) async-start(), calls=%async_computation.5 | async-start | bytes 3932160 | tf_op jit(solution)/shard_map/reduce_scatter | solution.py:160
  108.2 19.3 %slice-start = ((s8[16777216]{0:T(1024)(128)(4,1)}), s8[4194304]{0:T(1024)(128)(4,1)S(1)}, s32[]{:S(2)}) async-start(s8[16777216]{0:T(1024)(128)(4,1)} %bitcast.83), calls=%async_computation.6 | async-start | bytes 8388608
  108.2 19.3 %slice-start.1 = ((s8[16777216]{0:T(1024)(128)(4,1)}), s8[4194304]{0:T(1024)(128)(4,1)S(1)}, s32[]{:S(2)}) async-start(s8[16777216]{0:T(1024)(128)(4,1)} %bitcast.83), calls=%async_computation.7 | async-start | bytes 8388608
  117.7 9.8 %slice-start.2 = ((s8[16777216]{0:T(1024)(128)(4,1)}), s8[4194304]{0:T(1024)(128)(4,1)S(1)}, s32[]{:S(2)}) async-start(s8[16777216]{0:T(1024)(128)(4,1)} %bitcast.83), calls=%async_computation.8 | async-start | bytes 8388608
  117.7 9.8 %slice-start.3 = ((s8[16777216]{0:T(1024)(128)(4,1)}), s8[4194304]{0:T(1024)(128)(4,1)S(1)}, s32[]{:S(2)}) async-start(s8[16777216]{0:T(1024)(128)(4,1)} %bitcast.83), calls=%async_computation.9 | async-start | bytes 8388608
  142.0 0.9 copy-start.3
  142.0 1.1 copy-start.11
  142.0 1.8 copy-start.10
  142.0 1.9 copy-start.6
  142.1 18.7 %copy-start.13 = (bf16[512,256]{1,0:T(8,128)(2,1)S(1)}, bf16[512,256]{1,0:T(8,128)(2,1)}, u32[]{:S(2)}) copy-start(bf16[512,256]{1,0:T(8,128)(2,1)} %param.21) | copy-start | bytes 786436
  142.1 18.7 %copy-start.15 = (f32[512]{0:T(512)S(1)}, f32[512]{0:T(512)}, u32[]{:S(2)}) copy-start(f32[512]{0:T(512)} %param.20) | copy-start | bytes 6148
  160.2 0.6 copy-start.8
  164.6 0.7 copy-start.12
  165.2 0.8 copy-start.4
  165.2 0.8 copy-start.5
  168.0 25.1 %copy-start.9 = (f32[1024]{0:T(1024)S(1)}, f32[1024]{0:T(1024)}, u32[]{:S(2)}) copy-start(f32[1024]{0:T(1024)} %copy-done.8) | copy-start | bytes 12292
  168.0 25.1 %copy-start.14 = (bf16[512,256]{1,0:T(8,128)(2,1)S(1)}, bf16[512,256]{1,0:T(8,128)(2,1)}, u32[]{:S(2)}) copy-start(bf16[512,256]{1,0:T(8,128)(2,1)} %param.22) | copy-start | bytes 786436
  168.0 25.2 %copy-start.16 = (f32[512]{0:T(512)S(1)}, f32[512]{0:T(512)}, u32[]{:S(2)}) copy-start(f32[512]{0:T(512)} %param.20) | copy-start | bytes 6148
  186.2 25.6 %all-to-all-start.1 = ((bf16[8,48,1024]{2,1,0:T(8,128)(2,1)}), bf16[8,48,1024]{2,1,0:T(8,128)(2,1)S(1)}, u32[]{:S(2)}, u32[]{:S(2)}) async-start(bf16[8,48,1024]{2,1,0:T(8,128)(2,1)} %bitcast.89), calls=%async_computation.2 | async-start | bytes 1572864 | tf_op jit(solution)/shard_map/all_to_all | solution.py:167
  190.8 2.4 %copy-start.2 = (bf16[1024,512]{1,0:T(8,128)(2,1)S(1)}, bf16[1024,512]{1,0:T(8,128)(2,1)}, u32[]{:S(2)}) copy-start(bf16[1024,512]{1,0:T(8,128)(2,1)} %all-gather.3.cloned.1.call-done) | copy-start | bytes 3145732
  190.8 3.0 %copy-start.1 = (f32[4,128,1024]{2,1,0:T(8,128)S(1)}, f32[4,128,1024]{2,1,0:T(8,128)}, u32[]{:S(2)}) copy-start(f32[4,128,1024]{2,1,0:T(8,128)} %get-tuple-element.11) | copy-start | bytes 6291460
  193.9 9.9 %copy-start.7 = (f32[1024]{0:T(1024)S(1)}, f32[1024]{0:T(1024)}, u32[]{:S(2)}) copy-start(f32[1024]{0:T(1024)} %param.25) | copy-start | bytes 12292
Sparse Core Ops, SparseCore 0:
  56.6 51.4 all-gather.4
  109.8 22.2 all-gather.2
  142.2 43.9 reduce-scatter.1
where the time goes:
time: 225 us; the launch traced here: 224 us
  waiting for transfers between devices  76.2 us (34%)
  blocking collectives  48.8 us (22%)
  local copies, waits for them, and re-layouts  34.5 us (15%)
  matrix products  30.9 us (14%)
  other arithmetic  14.7 us (7%)
  between operations  14.2 us (6%)
  starting transfers between devices  4.91 us (2%)
    all_gather x1, waiting for transfers between devices, shards(): piece = lax.all_gather(arrived_part, 'tp', axis=3, tiled=True)  50.7 us
    all_to_all x1, blocking collectives, shards(): lax.all_to_all(my_columns, 'ep', split_axis=0, concat_axis=0, tiled=True)  27.1 us
    reduce_scatter x1, waiting for transfers between devices, shards(): lax.psum_scatter(term.reshape(lax.axis_size('tp') * out_cols, -1).astype(...  18.2 us
    all_gather x1, blocking collectives, shards(): lax.all_gather(rope_key, 'ep', axis=0, tiled=True)  12.8 us
    convert_element_type x2, local copies, waits for them, and re-layouts, shards(): term.reshape(lax.axis_size('tp') * out_cols, -1).astype(jnp.bfloat16)  10.2 us
    dot_general x1, matrix products, shards(): jnp.einsum('secd,edf->secf', piece, w_up, preferred_element_type=jnp.floa...  9.73 us
    gather x2, local copies, waits for them, and re-layouts, shards(): normed[slot_token]  9.56 us
    dot_general x1, matrix products, shards(): jnp.einsum('secd,edf->secf', piece, w_gate, preferred_element_type=jnp.fl...  9.51 us
  transfers between devices with their start and end apart: 4, of which 3 were waited for; matrix products, arithmetic and copies ran while one was open for 22% of the time, Pallas kernels for 0%

commit v1 on v0

--- a/solution.py
+++ b/solution.py
@@ -1,6 +1,11 @@
+import functools
+
 import jax
 import jax.numpy as jnp
+import numpy as np
 from jax import lax
+from jax.experimental import pallas as pl
+from jax.experimental.pallas import tpu as pltpu
 from jax.sharding import PartitionSpec as P
 
 NOPE = 64
@@ -8,6 +13,8 @@
 VDIM = 64
 QKD = 96
 CAP = 12
+TOP = 2
+PER_GROUP = 8
 
 
 EPS = 1e-06
@@ -172,6 +179,748 @@
     return (mixed, expert_out)
 
 
+BF16 = jnp.bfloat16
+F32 = jnp.float32
+ANY = pl.BlockSpec(memory_space=pl.ANY)
+WHOLE = pl.BlockSpec(memory_space=pltpu.VMEM)
+META = 128
+
+
+def iota(shape, dim):
+    return lax.broadcasted_iota(jnp.int32, shape, dim)
+
+
+def dot(left, right):
+    return jnp.dot(left, right, preferred_element_type=F32)
+
+
+def dot_nt(left, right):
+    return lax.dot_general(left, right, (((1,), (1,)), ((), ())), preferred_element_type=F32)
+
+
+def one_if(condition):
+    return jnp.where(condition, 1.0, 0.0).astype(BF16)
+
+
+def cost(flops, in_bytes):
+    return pl.CostEstimate(flops=int(flops), bytes_accessed=int(in_bytes), transcendentals=0)
+
+
+def limits(mib):
+    return pltpu.CompilerParams(vmem_limit_bytes=mib * 1024 * 1024)
+
+
+def in_hbm(values):
+    return pltpu.with_memory_space_constraint(values, pltpu.HBM)
+
+
+def start_all(pairs, sems):
+    copies = [pltpu.make_async_copy(src, dst, sems.at[i]) for i, (src, dst) in enumerate(pairs)]
+    for copy in copies:
+        copy.start()
+    return copies
+
+
+def wait_all(copies):
+    for copy in copies:
+        copy.wait()
+
+
+def dispatch_kernel(
+    chips, experts, slots, x_hbm, gain_hbm, ids_hbm, route_hbm, *refs
+):
+    outs, (x_ref, gain_ref, ids_ref, route_ref, sems) = refs[:-5], refs[-5:]
+    pairs = [(ids_hbm, ids_ref), (route_hbm, route_ref), (x_hbm, x_ref), (gain_hbm, gain_ref)]
+    copies = start_all(pairs, sems)
+    rows = x_ref.shape[0]
+    width = outs[0].shape[1] - META
+    sources, pick_ref = outs[:chips], outs[chips]
+    chip = lax.shift_right_logical(lax.axis_index("ep"), 1)
+    copies[0].wait()
+    copies[1].wait()
+    first, second = ids_ref[0:1, :], ids_ref[1:2, :]
+    group = lax.shift_right_logical(first, jnp.int32(PER_GROUP.bit_length() - 1))
+    target = group - chip
+    target = jnp.where(target < 0, target + chips, target)
+    places = iota((META, rows), 0)
+    hot_first, hot_second = places == first, places == second
+    hot_target = places == target + experts
+    earlier = one_if(iota((rows, rows), 0) < iota((rows, rows), 1))
+    counts = dot(one_if(hot_first | hot_second | hot_target), earlier)
+
+    def at(mask):
+        return jnp.sum(jnp.where(mask, counts, 0.0), axis=0, keepdims=True)
+
+    slot = target.astype(F32) * slots + at(hot_target)
+    values = [(first - group * PER_GROUP + 1).astype(F32), at(hot_first)]
+    values += [(second - group * PER_GROUP + 1).astype(F32), at(hot_second)]
+    for k in range(TOP):
+        weight = route_ref[k : k + 1, :]
+        high = weight.astype(BF16).astype(F32)
+        middle = (weight - high).astype(BF16).astype(F32)
+        values += [high, middle, weight - high - middle]
+    meta = jnp.zeros((META, rows), F32)
+    for place, value in enumerate(values):
+        meta = jnp.where(places == place, value, meta)
+    on_diagonal = iota((rows, rows), 0) == iota((rows, rows), 1)
+    slot_col = jnp.sum(jnp.where(on_diagonal, slot, 0.0), axis=1, keepdims=True)
+    pick_ref[...] = one_if(iota((rows, chips * slots), 1).astype(F32) == slot_col)
+    select = one_if(iota((chips * slots, rows), 0).astype(F32) == slot)
+    meta_rows = dot_nt(select, meta.astype(BF16)).astype(BF16)
+    for k in range(chips):
+        sources[k][:, width:] = meta_rows[k * slots : (k + 1) * slots]
+    copies[2].wait()
+    copies[3].wait()
+    stream = x_ref[...].astype(F32)
+    inverse = lax.rsqrt(jnp.mean(stream * stream, axis=-1, keepdims=True) + EPS)
+    columns = pl.ds(pl.multiple_of(lax.axis_index("tp") * width, 128), width)
+    part = x_ref[:, columns].astype(F32) * inverse * gain_ref[:, columns]
+    picked = dot(select, part.astype(BF16)).astype(BF16)
+    for k in range(chips):
+        sources[k][:, :width] = picked[k * slots : (k + 1) * slots]
+
+
+def scratch_like(*arrays):
+    return [pltpu.VMEM(a.shape, a.dtype) for a in arrays] + [pltpu.SemaphoreType.DMA((len(arrays),))]
+
+
+def make_dispatch(moe_input, moe_gain, expert_ids, route_weights, chips, experts, slots, width):
+    rows = moe_input.shape[0]
+    shapes = [jax.ShapeDtypeStruct((slots, width + META), BF16)] * chips
+    shapes += [jax.ShapeDtypeStruct((rows, chips * slots), BF16)]
+    arrays = (moe_input, moe_gain[None], expert_ids.T, route_weights.T)
+    outs = pl.pallas_call(
+        functools.partial(dispatch_kernel, chips, experts, slots),
+        out_shape=shapes,
+        in_specs=[ANY] * 4,
+        out_specs=[WHOLE] * len(shapes),
+        scratch_shapes=scratch_like(*arrays),
+        compiler_params=limits(16),
+        cost_estimate=cost(2e9, 4e6),
+        name="dispatch",
+    )(*[in_hbm(a) for a in arrays])
+    return outs[:chips], outs[chips]
+
+
+def stack_kernel(widths, count, *refs):
+    blocks, outs = refs[:count], refs[count + 1 :]
+    size = blocks[0].shape[0]
+    for k, block in enumerate(blocks):
+        first = 0
+        for out, width in zip(outs, widths):
+            out[k * size : (k + 1) * size, :] = block[:, first : first + width]
+            first += width
+
+
+def stack_blocks(blocks, widths, after):
+    rows = len(blocks) * blocks[0].shape[0]
+    return pl.pallas_call(
+        functools.partial(stack_kernel, widths, len(blocks)),
+        out_shape=[jax.ShapeDtypeStruct((rows, width), blocks[0].dtype) for width in widths],
+        in_specs=[WHOLE] * len(blocks) + [ANY],
+        out_specs=[WHOLE] * len(widths),
+        compiler_params=limits(8),
+        cost_estimate=cost(2e8, 1e6),
+        name="stack_blocks",
+    )(*blocks, after)
+
+
+def up_pairs(wg, wu, out, which, first=0):
+    count, width, hidden = out.shape[0], out.shape[1], wg.shape[2]
+    rows = pl.ds(pl.multiple_of((lax.axis_index("tp") ^ which) * width, 128), width)
+    pairs = []
+    for e in range(count):
+        pairs.append((wg.at[first + e, rows, :], out.at[e, :, pl.ds(0, hidden)]))
+        pairs.append((wu.at[first + e, rows, :], out.at[e, :, pl.ds(hidden, hidden)]))
+    return pairs
+
+
+def down_pairs(wd, out, which):
+    local, depth, width = wd.shape[0], wd.shape[1], out.shape[1]
+    columns = pl.ds(pl.multiple_of((lax.axis_index("tp") ^ which) * width, 128), width)
+    return [(wd.at[e, :, columns], out.at[pl.ds(e * depth, depth), :]) for e in range(local)]
+
+
+def hold_up_kernel(wg, wu, after, near_x, near_y, sems):
+    pairs = up_pairs(wg, wu, near_x, 1) + up_pairs(wg, wu, near_y, 2)
+    wait_all(start_all(pairs, sems))
+
+
+def hold_up(w_gate, w_up, width, after):
+    local, columns = w_gate.shape[0], 2 * w_gate.shape[2]
+    return pl.pallas_call(
+        hold_up_kernel,
+        out_shape=[
+            jax.ShapeDtypeStruct((local, width, columns), BF16),
+            jax.ShapeDtypeStruct((local // 2, width, columns), BF16),
+        ],
+        in_specs=[ANY] * 3,
+        out_specs=[WHOLE] * 2,
+        scratch_shapes=[pltpu.SemaphoreType.DMA((3 * local,))],
+        compiler_params=limits(2),
+        cost_estimate=cost(5e9, 3.4e7),
+        name="hold_up",
+    )(in_hbm(w_gate), in_hbm(w_up), after)
+
+
+def first_kernel(
+    chips, slots, local, xm, xt, mm, mt, wg, wu, acc, sel, back, weight, near_y, buf,
+    own_sems, sems,
+):
+    pairs = up_pairs(wg, wu, buf, 0)
+    start_all(pairs, own_sems)
+    others = start_all(up_pairs(wg, wu, near_y, 2, local - near_y.shape[0]), sems)
+    per_block, half = 2 * chips * CAP, chips * slots
+    core = (lax.axis_index("ep") & 1).astype(F32)
+    unit = one_if(iota((16, META), 0) == iota((16, META), 1))
+    total = jnp.zeros((local * per_block, 1), F32)
+    for side, meta_ref in ((0, mm), (1, mt)):
+        meta = meta_ref[...]
+        turned = dot_nt(unit, meta)
+        cols = meta.astype(F32)
+
+        def slot_of(take, block, k):
+            expert = take(2 * k) - 1.0 - core * local
+            inside = (expert >= 0.0) & (expert < local)
+            return jnp.where(inside, expert * per_block + block * CAP + take(2 * k + 1), -1.0)
+
+        def block_of(shape, dim):
+            place = iota(shape, dim)
+            block = jnp.full(shape, side * chips, jnp.int32)
+            for k in range(1, chips):
+                block = block + jnp.where(place >= k * slots, 1, 0)
+            return block.astype(F32)
+
+        def row_value(k):
+            return turned[k : k + 1, :]
+
+        def col_value(k):
+            return cols[:, k : k + 1]
+
+        places = iota((local * per_block, half), 0).astype(F32)
+        hits = [places == slot_of(row_value, block_of((1, half), 1), k) for k in range(TOP)]
+        for k in range(TOP):
+            base = 2 * TOP + 3 * k
+            share = row_value(base) + row_value(base + 1) + row_value(base + 2)
+            total += jnp.sum(jnp.where(hits[k], share, 0.0), axis=-1, keepdims=True)
+        sel[side] = one_if(hits[0] | hits[1])
+        wanted = [slot_of(col_value, block_of((half, 1), 0), k) for k in range(TOP)]
+        lanes = iota((half, local * per_block), 1).astype(F32)
+        back[side] = one_if((lanes == wanted[0]) | (lanes == wanted[1]))
+    weight[...] = jnp.broadcast_to(total, weight.shape)
+
+    @pl.loop(0, local)
+    def _(e):
+        picked = picked_rows(sel, e, per_block, xm, xt)
+        for j in range(2):
+            pltpu.make_async_copy(*pairs[j], own_sems.at[2 * e + j]).wait()
+        acc[e] = dot(picked, buf[e])
+
+    wait_all(others)
+
+
+def picked_rows(sel, e, count, mine, twin):
+    own = pl.ds(pl.multiple_of(e * count, 16), count)
+    return (dot(sel[0, own, :], mine[...]) + dot(sel[1, own, :], twin[...])).astype(BF16)
+
+
+def first_quarter(xm, xt, mm, mt, w_gate, w_up, chips, slots):
+    local, hidden, width = w_gate.shape[0], w_gate.shape[2], xm.shape[1]
+    per_block, half = 2 * chips * CAP, chips * slots
+    shapes = [
+        jax.ShapeDtypeStruct((local, per_block, 2 * hidden), F32),
+        jax.ShapeDtypeStruct((2, local * per_block, half), BF16),
+        jax.ShapeDtypeStruct((2, half, local * per_block), BF16),
+        jax.ShapeDtypeStruct((local * per_block, META), F32),
+        jax.ShapeDtypeStruct((local - local // 2, width, 2 * hidden), BF16),
+    ]
+    return pl.pallas_call(
+        functools.partial(first_kernel, chips, slots, local),
+        out_shape=shapes,
+        in_specs=[WHOLE] * 4 + [ANY] * 2,
+        out_specs=[WHOLE] * 5,
+        scratch_shapes=[
+            pltpu.VMEM((local, width, 2 * hidden), BF16),
+            pltpu.SemaphoreType.DMA((2 * local,)),
+            pltpu.SemaphoreType.DMA((2 * (local - local // 2),)),
+        ],
+        compiler_params=limits(12),
+        cost_estimate=cost(3e9, 1e7),
+        name="first_quarter",
+    )(xm, xt, mm, mt, in_hbm(w_gate), in_hbm(w_up))
+
+
+def beside_kernel(xm, xt, ym, yt, sel, start, near_x, low_y, high_y, wg, wu, wd, acc, far, down, *sems):
+    copies = start_all(up_pairs(wg, wu, far, 3), sems[0])
+    copies += start_all(down_pairs(wd, down, 3), sems[1])
+    _, per_block = start.shape[:2]
+    count = low_y.shape[0]
+
+    @pl.loop(0, count)
+    def _(i):
+        for e, y_ref in ((i, low_y), (i + count, high_y)):
+            both = start[e] + dot(picked_rows(sel, e, per_block, xm, xt), near_x[e])
+            acc[e] = both + dot(picked_rows(sel, e, per_block, ym, yt), y_ref[i])
+
+    wait_all(copies)
+
+
+def beside_quarters(xm, xt, ym, yt, sel, start, near_x, low_y, high_y, w_gate, w_up, w_down):
+    local, width = near_x.shape[:2]
+    return pl.pallas_call(
+        beside_kernel,
+        out_shape=[
+            jax.ShapeDtypeStruct(start.shape, F32),
+            jax.ShapeDtypeStruct(near_x.shape, BF16),
+            jax.ShapeDtypeStruct((local * w_down.shape[1], width), BF16),
+        ],
+        in_specs=[WHOLE] * 9 + [ANY] * 3,
+        out_specs=[WHOLE] * 3,
+        scratch_shapes=[
+            pltpu.SemaphoreType.DMA((2 * local,)),
+            pltpu.SemaphoreType.DMA((local,)),
+        ],
+        compiler_params=limits(4),
+        cost_estimate=cost(3e9, 1e7),
+        name="beside_quarters",
+    )(
+        xm, xt, ym, yt, sel, start, near_x, low_y, high_y, in_hbm(w_gate), in_hbm(w_up),
+        in_hbm(w_down),
+    )
+
+
+def far_kernel(m0, m1, t0, t1, sel, weight, start, far, wd, out, down_x, down_y, xm, xt, *sems):
+    copies = start_all(down_pairs(wd, down_x, 1), sems[0])
+    copies += start_all(down_pairs(wd, down_y, 2), sems[1])
+    local, hidden = start.shape[0], start.shape[2] // 2
+    per_block, half = start.shape[1], sel.shape[2]
+    for whole, parts in ((xm, (m0, m1)), (xt, (t0, t1))):
+        whole[: half // 2, :] = parts[0][...]
+        whole[half // 2 :, :] = parts[1][...]
+
+    @pl.loop(0, local // 2)
+    def _(i):
+        for e in (2 * i, 2 * i + 1):
+            mine = pl.ds(pl.multiple_of(e * per_block, 16), per_block)
+            both = start[e] + dot(picked_rows(sel, e, per_block, xm, xt), far[e])
+            gate = both[:, :hidden]
+            act = gate / (1.0 + jnp.exp(-gate)) * both[:, hidden:] * weight[mine, 0:1]
+            out[mine, :] = act.astype(BF16)
+
+    wait_all(copies)
+
+
+def far_quarter(m0, m1, t0, t1, sel, weight, start, far, w_down):
+    local, hidden, width, half = start.shape[0], start.shape[2] // 2, m0.shape[1], sel.shape[2]
+    down = jax.ShapeDtypeStruct((local * w_down.shape[1], width), BF16)
+    return pl.pallas_call(
+        far_kernel,
+        out_shape=[jax.ShapeDtypeStruct((sel.shape[1], hidden), BF16), down, down],
+        in_specs=[WHOLE] * 8 + [ANY],
+        out_specs=[WHOLE] * 3,
+        scratch_shapes=[pltpu.VMEM((half, width), BF16)] * 2
+        + [pltpu.SemaphoreType.DMA((local,))] * 2,
+        compiler_params=limits(6),
+        cost_estimate=cost(3e9, 1e7),
+        name="far_quarter",
+    )(m0, m1, t0, t1, sel, weight, start, far, in_hbm(w_down))
+
+
+def split_kernel(x_ref, y_ref, first, second):
+    rows = first.shape[0]
+    first[...] = x_ref[:rows, :]
+    second[...] = y_ref[rows:, :]
+
+
+def split_halves(x_block, y_block):
+    half = jax.ShapeDtypeStruct((x_block.shape[0] // 2, x_block.shape[1]), BF16)
+    return pl.pallas_call(
+        split_kernel,
+        out_shape=[half, half],
+        in_specs=[WHOLE] * 2,
+        out_specs=[WHOLE] * 2,
+        compiler_params=limits(4),
+        cost_estimate=cost(1e8, 1e6),
+        name="split_halves",
+    )(x_block, y_block)
+
+
+def down_kernel(local, acts, back, wd, mine, twin, held):
+    count, depth = acts.shape[0] // local, acts.shape[1]
+    for e in range(local):
+        rows = pl.ds(e * count, count)
+        held[rows, :] = dot(acts[rows, :], wd[e * depth : (e + 1) * depth, :]).astype(BF16)
+    twin[...] = dot(back[1], held[...]).astype(BF16)
+    mine[...] = dot(back[0], held[...])
+
+
+def down_quarter(acts, back, wd):
+    half, width = back.shape[1], wd.shape[1]
+    return pl.pallas_call(
+        functools.partial(down_kernel, wd.shape[0] // acts.shape[1]),
+        out_shape=[
+            jax.ShapeDtypeStruct((half, width), F32),
+            jax.ShapeDtypeStruct((half, width), BF16),
+        ],
+        in_specs=[WHOLE] * 3,
+        out_specs=[WHOLE] * 2,
+        scratch_shapes=[pltpu.VMEM((acts.shape[0], width), BF16)],
+        compiler_params=limits(4),
+        cost_estimate=cost(1.8e9, 6e6),
+        name="down_quarter",
+    )(acts, back, wd)
+
+
+def sum_kernel(first, mine, twin, *refs):
+    extras, out = refs[:-1], refs[-1]
+    rows = pl.ds(first, out.shape[0])
+    total = mine[rows, :] + twin[rows, :].astype(F32)
+    for extra in extras:
+        total += extra[...].astype(F32)
+    out[...] = total.astype(BF16)
+
+
+def sum_half(second, mine, twin, *extras):
+    rows = mine.shape[0] // 2
+    return pl.pallas_call(
+        functools.partial(sum_kernel, rows * second),
+        out_shape=jax.ShapeDtypeStruct((rows, mine.shape[1]), BF16),
+        in_specs=[WHOLE] * (2 + len(extras)),
+        out_specs=WHOLE,
+        compiler_params=limits(4),
+        cost_estimate=cost(2e8, 1e6),
+        name="sum_half",
+    )(mine, twin, *extras)
+
+
+def join_kernel(first, slots, own, twin, x_part, y_part, *outs):
+    for k, out in enumerate(outs):
+        near = pl.ds(k * slots, slots)
+        rows = pl.ds(first + k * slots, slots)
+        total = own[rows, :] + twin[rows, :].astype(F32)
+        out[...] = (total + x_part[near, :].astype(F32) + y_part[near, :].astype(F32)).astype(BF16)
+
+
+def join_half(second, own, twin, x_part, y_part, slots):
+    rows, width = x_part.shape
+    return pl.pallas_call(
+        functools.partial(join_kernel, second * rows, slots),
+        out_shape=[jax.ShapeDtypeStruct((slots, width), BF16)] * (rows // slots),
+        in_specs=[WHOLE] * 4,
+        out_specs=[WHOLE] * (rows // slots),
+        compiler_params=limits(4),
+        cost_estimate=cost(3e8, 2e6),
+        name="join_half",
+    )(own, twin, x_part, y_part)
+
+
+def place_kernel(pick, *refs):
+    blocks, out, held = refs[:-2], refs[-2], refs[-1]
+    slots = blocks[0].shape[0]
+    for k, block in enumerate(blocks):
+        held[k * slots : (k + 1) * slots, :] = block[...]
+    out[...] = dot(pick[...], held[...]).astype(BF16)
+
+
+def place_rows(pick, blocks):
+    width = blocks[0].shape[1]
+    return pl.pallas_call(
+        place_kernel,
+        out_shape=jax.ShapeDtypeStruct((pick.shape[0], width), BF16),
+        in_specs=[WHOLE] * (1 + len(blocks)),
+        out_specs=WHOLE,
+        scratch_shapes=[pltpu.VMEM((pick.shape[1], width), BF16)],
+        compiler_params=limits(16),
+        cost_estimate=cost(5e8, 1e6),
+        name="place_rows",
+    )(pick, *blocks)
+
+
+def head_masks(heads, shape):
+    lanes = iota(shape, 1)
+    edge = heads * NOPE
+    masks = []
+    for h in range(heads):
+        nope = (lanes >= h * NOPE) & (lanes < (h + 1) * NOPE)
+        turned = (lanes >= edge + h * ROPE) & (lanes < edge + (h + 1) * ROPE)
+        masks.append(nope | turned)
+    return masks
+
+
+def attend_prep_kernel(heads, count, *refs):
+    sources, (after, kv, stacked) = refs[:count], refs[count : count + 3]
+    held, sems = refs[count + 3 : -1], refs[-1]
+    for copy in start_all(list(zip(sources, held)), sems):
+        copy.wait()
+    latent, rope, lat_gain, key_up, value_up, queries, q_gain, k_gain, rates, q_map, k_map, g_map = held
+    nope, turned = heads * NOPE, heads * ROPE
+    rows = latent.shape[0]
+    position = iota((rows, turned), 0) + lax.axis_index("ep") * rows
+    angles = position.astype(F32) * rates[...]
+    cos, sin = jnp.cos(angles), jnp.sin(angles)
+    masks = head_masks(heads, (rows, nope + turned))
+    place = iota((8, QKD), 0)
+    split = jnp.zeros((8, QKD), F32)
+    for i, gain in enumerate((q_gain, k_gain)):
+        whole = gain[...]
+        high = whole.astype(BF16).astype(F32)
+        middle = (whole - high).astype(BF16).astype(F32)
+        for j, piece in enumerate((high, middle, whole - high - middle)):
+            split = jnp.where(place == 3 * i + j, piece, split)
+    spread = dot(split.astype(BF16), g_map[...])
+    gains = [spread[i : i + 1] + spread[i + 1 : i + 2] + spread[i + 2 : i + 3] for i in (0, 3)]
+
+    def finish(values, pair, inverse, gain):
+        low = values[:, :nope] * inverse[:, :nope] * gain[:, :nope]
+        high = values[:, nope:] * gain[:, nope : nope + turned] * cos
+        high = (high + pair * gain[:, nope + turned :] * sin) * inverse[:, nope:]
+        return low, high
+
+    both = dot(queries[...], q_map[...])
+    values, pair = both[:, : nope + turned], both[:, nope + turned :]
+    squares = values * values
+    inverse = jnp.zeros(values.shape, F32)
+    for mask in masks:
+        total = jnp.sum(jnp.where(mask, squares, 0.0), axis=-1, keepdims=True)
+        inverse = jnp.where(mask, lax.rsqrt(total / QKD + EPS), inverse)
+    low, high = finish(values, pair, inverse, gains[0])
+    for h in range(heads):
+        mine = pl.ds(h * rows, rows)
+        stacked[mine, :nope] = jnp.where(masks[h][:, :nope], low, 0.0).astype(BF16)
+        stacked[mine, nope:] = jnp.where(masks[h][:, nope:], high, 0.0).astype(BF16)
+
+    lat = latent[...].astype(F32)
+    scale = lax.rsqrt(jnp.mean(lat * lat, axis=-1, keepdims=True) + EPS)
+    normed = (lat * scale * lat_gain[...]).astype(BF16)
+    key_nope = dot(normed, key_up[...]).astype(BF16).astype(F32)
+    shared = lax.dot_general(
+        rope[...], k_map[...], (((0,), (0,)), ((), ())), preferred_element_type=F32
+    )
+    turned_k, pair_k = shared[:, :turned], shared[:, turned:]
+    values = jnp.concatenate([key_nope, turned_k], axis=1)
+    squares = values * values
+    inverse = jnp.zeros(values.shape, F32)
+    for mask in masks:
+        total = jnp.sum(jnp.where(mask, squares, 0.0), axis=-1, keepdims=True)
+        inverse = jnp.where(mask, lax.rsqrt(total / QKD + EPS), inverse)
+    low, high = finish(values, pair_k, inverse, gains[1])
+    kv[:, :nope] = low.astype(BF16)
+    kv[:, nope : nope + turned] = high.astype(BF16)
+    kv[:, nope + turned :] = dot(normed, value_up[...]).astype(BF16)
+
+
+def rope_maps(heads):
+    half = ROPE // 2
+    nope, turned = heads * NOPE, heads * ROPE
+    q_map = np.zeros((heads * QKD, nope + 2 * turned), np.float32)
+    k_map = np.zeros((ROPE, 2 * turned), np.float32)
+    g_map = np.zeros((QKD, nope + 2 * turned), np.float32)
+    for h in range(heads):
+        for i in range(NOPE):
+            q_map[h * QKD + i, h * NOPE + i] = 1
+        for i in range(ROPE):
+            other, sign = (i + half, -1) if i < half else (i - half, 1)
+            at = h * ROPE + i
+            q_map[h * QKD + NOPE + i, nope + at] = 1
+            q_map[h * QKD + NOPE + other, nope + turned + at] = sign
+            k_map[i, at] = 1
+            k_map[other, turned + at] = sign
+        g_map += np.abs(q_map[h * QKD : (h + 1) * QKD])
+    rates = np.tile(np.float32(THETA) ** (-np.arange(half, dtype=np.float32) / half), turned // half)
+    return [jnp.asarray(rates[None], F32)] + [jnp.asarray(m, BF16) for m in (q_map, k_map, g_map)]
+
+
+def attend_prep(latent, rope, lat_gain, key_up, value_up, queries, query_gain, key_gain, after):
+    rows, heads = latent.shape[0], key_up.shape[1] // NOPE
+    wide = heads * (NOPE + ROPE)
+    arrays = [latent, rope.T, lat_gain[None], key_up, value_up, queries]
+    arrays += [query_gain[None], key_gain[None]] + rope_maps(heads)
+    return pl.pallas_call(
+        functools.partial(attend_prep_kernel, heads, len(arrays)),
+        out_shape=[
+            jax.ShapeDtypeStruct((rows, wide + heads * VDIM), BF16),
+            jax.ShapeDtypeStruct((heads * rows, wide), BF16),
+        ],
+        in_specs=[ANY] * (len(arrays) + 1),
+        out_specs=[WHOLE] * 2,
+        scratch_shapes=scratch_like(*arrays),
+        compiler_params=limits(8),
+        cost_estimate=cost(2e9, 4e6),
+        name="attend_prep",
+    )(*[in_hbm(a) for a in arrays], after)
+
+
+def attend_kernel(heads, chips, stacked, mine, twin, wd, out, down, held, mixed, sems):
+    copies = start_all(down_pairs(wd, down, 0), sems)
+    rows = out.shape[0]
+    width = heads * (NOPE + ROPE)
+    core = lax.axis_index("ep") & 1
+    chip = lax.shift_right_logical(lax.axis_index("ep"), 1)
+    place = iota((heads * rows, 1), 0)
+    for h in range(1, heads):
+        place = place - jnp.where(iota((heads * rows, 1), 0) >= h * rows, rows, 0)
+    query_pos = place + lax.axis_index("ep") * rows
+
+    @pl.loop(0, chips)
+    def _(back):
+        where = pl.ds(pl.multiple_of(back * rows, 128), rows)
+        for side, keys in ((0, mine), (1, twin)):
+            source = (chip - back) * 2 + (core if side == 0 else 1 - core)
+            first = jnp.where(chip >= back, source * rows, 1 << 30)
+            scores = dot_nt(stacked[...], keys[where, :width]) * (QKD ** (-0.5))
+            seen = iota((heads * rows, rows), 1) + first <= query_pos
+            lanes = pl.ds(pl.multiple_of((side * chips + back) * rows, 128), rows)
+            held[:, lanes] = jnp.where(seen, scores, -1e30)
+
+    mixed[...] = jnp.zeros(mixed.shape, F32)
+    size = chips * rows
+    lanes = iota((rows, heads * VDIM), 1)
+
+    @pl.loop(0, heads // 2)
+    def _(i):
+        for h in (2 * i, 2 * i + 1):
+            scores = held[pl.ds(pl.multiple_of(h * rows, 128), rows), :]
+            expo = jnp.exp(scores - jnp.max(scores, axis=-1, keepdims=True))
+            total = jnp.sum(expo, axis=-1, keepdims=True)
+            probs = expo.astype(BF16)
+            result = dot(probs[:, :size], mine[:, width:]) + dot(probs[:, size:], twin[:, width:])
+            own = (lanes >= h * VDIM) & (lanes < (h + 1) * VDIM)
+            mixed[...] += jnp.where(own, result / total, 0.0)
+
+    out[...] = mixed[...].astype(BF16)
+    wait_all(copies)
+
+
+def attend(stacked, mine, twin, w_down, width, heads, chips):
+    rows, local = stacked.shape[0] // heads, w_down.shape[0]
+    return pl.pallas_call(
+        functools.partial(attend_kernel, heads, chips),
+        out_shape=[
+            jax.ShapeDtypeStruct((rows, heads * VDIM), BF16),
+            jax.ShapeDtypeStruct((local * w_down.shape[1], width), BF16),
+        ],
+        in_specs=[WHOLE] * 3 + [ANY],
+        out_specs=[WHOLE] * 2,
+        scratch_shapes=[
+            pltpu.VMEM((heads * rows, 2 * chips * rows), F32),
+            pltpu.VMEM((rows, heads * VDIM), F32),
+            pltpu.SemaphoreType.DMA((local,)),
+        ],
+        compiler_params=limits(12),
+        cost_estimate=cost(5e9, 4e6),
+        name="attend",
+    )(stacked, mine, twin, in_hbm(w_down))
+
+
+def project_kernel(gain, proj, *refs):
+    parts, out = refs[:-1], refs[-1]
+    depth = parts[0].shape[1]
+    total = jnp.zeros(out.shape, F32)
+    squares = jnp.zeros((out.shape[0], 1), F32)
+    for j, part in enumerate(parts):
+        rows = pl.ds(pl.multiple_of((lax.axis_index("tp") ^ j) * depth, 128), depth)
+        value = part[...].astype(F32)
+        squares += jnp.sum(value * value, axis=-1, keepdims=True)
+        total += dot((value * gain[:, rows]).astype(BF16), proj[rows, :])
+    out[...] = (total * lax.rsqrt(squares / (depth * len(parts)) + EPS)).astype(BF16)
+
+
+def project(gain, proj, parts):
+    return pl.pallas_call(
+        project_kernel,
+        out_shape=jax.ShapeDtypeStruct((parts[0].shape[0], proj.shape[1]), BF16),
+        in_specs=[WHOLE] * (2 + len(parts)),
+        out_specs=WHOLE,
+        compiler_params=limits(16),
+        cost_estimate=cost(1e9, 3e6),
+        name="project",
+    )(gain[None], proj, *parts)
+
+
+def twin_shards(
+    queries, kv_latent, rope_key, latent_gain, key_up, value_up, query_gain, key_gain, out_gain,
+    out_proj, moe_input, moe_gain, expert_ids, route_weights, w_gate, w_up, w_down,
+):
+    ep, tp = lax.axis_size("ep"), lax.axis_size("tp")
+    chips, experts = ep // 2, ep * w_gate.shape[0]
+    slots = PER_GROUP * CAP // TOP
+    width = moe_input.shape[1] // tp
+    heads = key_up.shape[1] // NOPE
+
+    def send(values, axis, pairs):
+        return lax.ppermute(values, axis, pairs)
+
+    def along(values, shift):
+        return send(values, "ep", [(i, (i + 2 * shift) % ep) for i in range(ep)])
+
+    def across(values):
+        return send(values, "ep", [(i, i ^ 1) for i in range(ep)])
+
+    def sideways(values, which):
+        return send(values, "tp", [(i, i ^ which) for i in range(tp)])
+
+    others, middle = range(1, chips), chips // 2
+    sources, pick = make_dispatch(
+        moe_input, moe_gain, expert_ids, route_weights, chips, experts, slots, width
+    )
+    arrived = [sources[0]] + [along(sources[k], k) for k in others]
+    near_x, low_y = hold_up(w_gate, w_up, width, pick)
+    kv, stacked = attend_prep(
+        kv_latent, rope_key, latent_gain, key_up, value_up, queries, query_gain,
+        key_gain, pick,
+    )
+    own, meta = stack_blocks(arrived, (width, META), near_x)
+    own_twin, meta_twin = across(own), across(meta)
+    x_block, y_block = sideways(own, 1), sideways(own, 2)
+    kv_blocks = [kv] + [along(kv, k) for k in others]
+    start, sel, back, weight, high_y = first_quarter(
+        own, own_twin, meta, meta_twin, w_gate, w_up, chips, slots
+    )
+    x_half, y_half = split_halves(x_block, y_block)
+    far_first, far_second = sideways(x_half, 2), sideways(y_half, 1)
+    x_twin, y_twin = across(x_block), across(y_block)
+    start, far_weights, down_d = beside_quarters(
+        x_block, x_twin, y_block, y_twin, sel, start, near_x, low_y, high_y,
+        w_gate, w_up, w_down,
+    )
+    twin_first, twin_second = across(far_first), across(far_second)
+    (kv_mine,) = stack_blocks(kv_blocks, (kv.shape[1],), kv)
+    kv_twin = across(kv_mine)
+    acts, down_x, down_y = far_quarter(
+        far_first, far_second, twin_first, twin_second, sel, weight, start,
+        far_weights, w_down,
+    )
+    d_mine, d_twin = down_quarter(acts, back, down_d)
+    d_twin = across(d_twin)
+    x_mine, x_twin = down_quarter(acts, back, down_x)
+    x_twin = across(x_twin)
+    from_y = sideways(sum_half(1, d_mine, d_twin), 2)
+    from_x = sideways(sum_half(0, d_mine, d_twin), 1)
+    y_mine, y_twin = down_quarter(acts, back, down_y)
+    y_twin = across(y_twin)
+    x_first = sideways(sum_half(0, x_mine, x_twin), 1)
+    y_second = sideways(sum_half(1, y_mine, y_twin), 2)
+    x_second = sideways(sum_half(1, x_mine, x_twin, from_y), 1)
+    y_first = sideways(sum_half(0, y_mine, y_twin, from_x), 2)
+    attn, down_own = attend(stacked, kv_mine, kv_twin, w_down, width, heads, chips)
+    mine, twin = down_quarter(acts, back, down_own)
+    twin = across(twin)
+    parts = [attn] + [sideways(attn, which) for which in range(1, tp)]
+    second = join_half(1, mine, twin, x_second, y_second, slots)
+    returned = [along(block, -k) for k, block in enumerate(second, middle)]
+    first = join_half(0, mine, twin, x_first, y_first, slots)
+    returned = [along(first[k], -k) for k in range(1, middle)] + returned
+    mixed = project(out_gain, out_proj, parts)
+    expert_out = place_rows(pick, [first[0]] + returned)
+    return (mixed, expert_out)
+
+
+def fits_twins(mesh, w_gate):
+    ep, tp = mesh.shape["ep"], mesh.shape["tp"]
+    local = w_gate.shape[0] // ep
+    return tp == 4 and ep % 4 == 0 and local % 2 == 0 and 2 * local == PER_GROUP and w_gate.shape[0] + ep // 2 <= META
+
+
 def solution(mesh):
     in_specs = (
         P("ep", "tp"),
@@ -193,4 +942,15 @@
         P("ep", "tp", None),
     )
     out_specs = (P("ep", "tp"), P("ep", "tp"))
-    return jax.shard_map(shards, mesh=mesh, in_specs=in_specs, out_specs=out_specs, check_vma=False)
+
+    def mapped(body):
+        return jax.shard_map(
+            body, mesh=mesh, in_specs=in_specs, out_specs=out_specs, check_vma=False
+        )
+
+    def step(*arrays):
+        if not fits_twins(mesh, arrays[14]):
+            return mapped(shards)(*arrays)
+        return mapped(twin_shards)(*arrays)
+
+    return step

time: 225 us -> 92.3 us (0.41)
  waiting for transfers between devices: 76.2 us -> 25.4 us
  blocking collectives: 48.8 us -> 0 us
  local copies, waits for them, and re-layouts: 34.5 us -> 0.01 us
  Pallas kernels: 0 us -> 32.2 us
  matrix products: 30.9 us -> 0 us
  starting transfers between devices: 4.91 us -> 33.6 us
  other arithmetic: 14.7 us -> 0 us
  between operations: 14.2 us -> 0.87 us
    all_gather x2 -> x0, waiting for transfers between devices: 50.7 us -> none  [the longest x1 50.7 us: shards(): piece = lax.all_gather(arrived_part, 'tp', axis=3, tiled=True)]
    ppermute x0 -> x33, starting transfers between devices: none -> 33.6 us  [send(): return lax.ppermute(values, axis, pairs)]
    pallas_call x0 -> x24, Pallas kernels: none -> 32.2 us  [the longest x1 5.34 us: first_quarter(): pl.pallas_call(functools.partial(first_kernel, chips, slots, local), out_...]
    dot_general x8 -> x0, matrix products: 30.9 us -> none  [the longest x1 9.73 us: shards(): jnp.einsum('secd,edf->secf', piece, w_up, preferred_element_type=jnp.floa...]
    all_to_all x1 -> x0, blocking collectives: 27.1 us -> none  [shards(): lax.all_to_all(my_columns, 'ep', split_axis=0, concat_axis=0, tiled=True)]
    ppermute x0 -> x33, waiting for transfers between devices: none -> 25.4 us  [send(): return lax.ppermute(values, axis, pairs)]
    all_gather x2 -> x0, blocking collectives: 21.7 us -> none  [the longest x1 12.8 us: shards(): lax.all_gather(rope_key, 'ep', axis=0, tiled=True)]
    reduce_scatter x1 -> x0, waiting for transfers between devices: 18.2 us -> none  [shards(): lax.psum_scatter(term.reshape(lax.axis_size('tp') * out_cols, -1).astype(...]
  transfers between devices with their start and end apart: 4 -> 33, of which waited for: 3 -> 12; matrix products, arithmetic and copies ran while one was open for 22% -> 0% of each run, Pallas kernels for 0% -> 32%
where the time goes in v1:
time: 92.3 us; the launch traced here: 92.1 us
  starting transfers between devices  33.6 us (36%)
  Pallas kernels  32.2 us (35%)
  waiting for transfers between devices  25.4 us (28%)
    ppermute x33, starting transfers between devices, send(): return lax.ppermute(values, axis, pairs)  33.6 us
    ppermute x33, waiting for transfers between devices, send(): return lax.ppermute(values, axis, pairs)  25.4 us
    pallas_call x1, Pallas kernels, first_quarter(): pl.pallas_call(functools.partial(first_kernel, chips, slots, local), out_...  5.34 us
    pallas_call x4, Pallas kernels, down_quarter(): pl.pallas_call(functools.partial(down_kernel, wd.shape[0] // acts.shape[1...  4.92 us
    pallas_call x1, Pallas kernels, beside_quarters(): pl.pallas_call(beside_kernel, out_shape=[jax.ShapeDtypeStruct(start.shape...  4.71 us
    pallas_call x1, Pallas kernels, hold_up(): pl.pallas_call(hold_up_kernel, out_shape=[jax.ShapeDtypeStruct((local, wi...  4.7 us
    pallas_call x1, Pallas kernels, far_quarter(): pl.pallas_call(far_kernel, out_shape=[jax.ShapeDtypeStruct((sel.shape[1],...  3.52 us
    pallas_call x1, Pallas kernels, attend(): pl.pallas_call(functools.partial(attend_kernel, heads, chips), out_shape=...  2.45 us
  transfers between devices with their start and end apart: 33, of which 12 were waited for; matrix products, arithmetic and copies ran while one was open for 0% of the time, Pallas kernels for 32%

profile of v1, /device:TPU:0, one launch (start us, length us, event | category | flops | bytes accessed | tf_op | source)
XLA Modules:
  0.0 92.1 jit_solution(10283631489538041112)
XLA Ops:
  0.6 1.8 %dispatch.1 = (bf16[48,1152]{1,0:T(8,128)(2,1)S(1)}, bf16[48,1152]{1,0:T(8,128)(2,1)S(1)}, bf16[48,1152]{1,0:T(8,128)(2,1)S(1)}, bf16[48,1152]{1,0:T(8,128)(2,1)S(1)}, bf16[128,192]{1,0:T(8,128)(2,1)S(1)}) custom-call(bf16[128,4096]{1,0:T(8,128)(2,1)} %x_hbm.1, f32[1,4096]{1,0:T(1,128)} %bitcast.9, s32[2,128]{1,0:T(2,128)} %bitcast.12, f32[2,128]{1,0:T(2,128)} %bitcast.13), custom_call_target="tpu_custom_call" | custom-call | flops 2000000000 | bytes 4000000 | tf_op jit(solution)/shard_map/dispatch/pallas_call | solution.py:292
  2.5 3.1 %collective-permute-start.7 = (bf16[48,1152]{1,0:T(8,128)(2,1)S(1)}, bf16[48,1152]{1,0:T(8,128)(2,1)S(1)}, u32[]{:S(2)}, u32[]{:S(2)}) collective-permute-start(bf16[48,1152]{1,0:T(8,128)(2,1)S(1)} %get-tuple-element.45), channel_id=1, source_target_pairs={{0,8},{4,12},{8,16},{12,20},{16,24},{20,28},{24,0},{28,4},{1,9},{5... | collective-permute-start | bytes 331784 | tf_op jit(solution)/shard_map/ppermute | solution.py:851
  5.6 2.6 %collective-permute-start.8 = (bf16[48,1152]{1,0:T(8,128)(2,1)S(1)}, bf16[48,1152]{1,0:T(8,128)(2,1)S(1)}, u32[]{:S(2)}, u32[]{:S(2)}) collective-permute-start(bf16[48,1152]{1,0:T(8,128)(2,1)S(1)} %get-tuple-element.46), channel_id=1, source_target_pairs={{0,16},{4,20},{8,24},{12,28},{16,0},{20,4},{24,8},{28,12},{1,17},{... | collective-permute-start | bytes 331784 | tf_op jit(solution)/shard_map/ppermute | solution.py:851
  8.2 1.3 %collective-permute-start.9 = (bf16[48,1152]{1,0:T(8,128)(2,1)S(1)}, bf16[48,1152]{1,0:T(8,128)(2,1)S(1)}, u32[]{:S(2)}, u32[]{:S(2)}) collective-permute-start(bf16[48,1152]{1,0:T(8,128)(2,1)S(1)} %get-tuple-element.47), channel_id=1, source_target_pairs={{0,24},{4,28},{8,0},{12,4},{16,8},{20,12},{24,16},{28,20},{1,25},{... | collective-permute-start | bytes 331784 | tf_op jit(solution)/shard_map/ppermute | solution.py:851
  9.5 4.7 %hold_up.1 = (bf16[4,1024,1024]{2,1,0:T(8,128)(2,1)S(1)}, bf16[2,1024,1024]{2,1,0:T(8,128)(2,1)S(1)}) custom-call(bf16[4,4096,512]{2,1,0:T(8,128)(2,1)} %wg.5, bf16[4,4096,512]{2,1,0:T(8,128)(2,1)} %wu.5, bf16[128,192]{1,0:T(8,128)(2,1)S(1)} %get-tuple-element.40.refs_12_.after.pick), custom_call_target="tpu_custom_call" | custom-call | flops 5000000000 | bytes 34000000 | tf_op jit(solution)/shard_map/hold_up/pallas_call | solution.py:351
  14.2 1.3 %collective-permute-done.8.refs_2_ = bf16[48,1152]{1,0:T(8,128)(2,1)S(1)} collective-permute-done((bf16[48,1152]{1,0:T(8,128)(2,1)S(1)}, bf16[48,1152]{1,0:T(8,128)(2,1)S(1)}, u32[]{:S(2)}, u32[]{:S(2)}) %collective-permute-start.8) | collective-permute-done | bytes 110624 | tf_op jit(solution)/shard_map/ppermute | solution.py:851
  15.6 1.6 %collective-permute-start.10 = (bf16[192,1024]{1,0:T(8,128)(2,1)S(1)}, bf16[192,1024]{1,0:T(8,128)(2,1)S(1)}, u32[]{:S(2)}, u32[]{:S(2)}) collective-permute-start(bf16[192,1024]{1,0:T(8,128)(2,1)S(1)} %get-tuple-element.49.xm), channel_id=1, source_target_pairs={{0,1},{1,0},{2,3},{3,2},{4,5},{5,4},{6,7},{7,6},{8,9},{9,8},{10,11... | collective-permute-start | bytes 1179656 | tf_op jit(solution)/shard_map/ppermute | solution.py:851
  17.2 1.5 %collective-permute-start.11 = (bf16[192,1024]{1,0:T(8,128)(2,1)S(1)}, bf16[192,1024]{1,0:T(8,128)(2,1)S(1)}, u32[]{:S(2)}, u32[]{:S(2)}) collective-permute-start(bf16[192,1024]{1,0:T(8,128)(2,1)S(1)} %get-tuple-element.49.xm), channel_id=1, source_target_pairs={{0,2},{1,3},{2,0},{3,1},{4,6},{5,7},{6,4},{7,5},{8,10},{9,11},{10,... | collective-permute-start | bytes 1179656 | tf_op jit(solution)/shard_map/ppermute | solution.py:851
  18.7 2.1 %attend_prep.1 = (bf16[128,640]{1,0:T(8,128)(2,1)S(1)}, bf16[512,384]{1,0:T(8,128)(2,1)S(1)}) custom-call(bf16[128,512]{1,0:T(8,128)(2,1)} %refs_0_.1, bf16[32,128]{1,0:T(8,128)(2,1)} %bitcast.10, f32[1,512]{1,0:T(1,128)} %bitcast.11, bf16[512,256]{1,0:T(8,128)(2,1)} %refs_3_.1, bf16[512,256]{1,0:T(8,128)(2,1)} %refs_4_.1, bf16[128,384]{1,0:T(8,128)(2,1)} %refs_5_.1, ...), custom_call_target="tpu_custom_call" | custom-call | flops 2000000000 | bytes 4000000 | tf_op jit(solution)/shard_map/attend_prep/pallas_call | solution.py:738
  20.9 2.9 %collective-permute-start = (bf16[128,640]{1,0:T(8,128)(2,1)S(1)}, bf16[128,640]{1,0:T(8,128)(2,1)S(1)}, u32[]{:S(2)}, u32[]{:S(2)}) collective-permute-start(bf16[128,640]{1,0:T(8,128)(2,1)S(1)} %get-tuple-element.42.refs_0_.refs_4_), channel_id=1, source_target_pairs={{0,8},{4,12},{8,16},{12,20},{16,24},{20,28},{24,0},{28,4},{1,9},{5... | collective-permute-start | bytes 491528 | tf_op jit(solution)/shard_map/ppermute | solution.py:851
  23.8 1.6 %collective-permute-start.1 = (bf16[128,640]{1,0:T(8,128)(2,1)S(1)}, bf16[128,640]{1,0:T(8,128)(2,1)S(1)}, u32[]{:S(2)}, u32[]{:S(2)}) collective-permute-start(bf16[128,640]{1,0:T(8,128)(2,1)S(1)} %get-tuple-element.42.refs_0_.refs_4_), channel_id=1, source_target_pairs={{0,16},{4,20},{8,24},{12,28},{16,0},{20,4},{24,8},{28,12},{1,17},{... | collective-permute-start | bytes 491528 | tf_op jit(solution)/shard_map/ppermute | solution.py:851
  25.3 4.6 %collective-permute-done.refs_1_ = bf16[128,640]{1,0:T(8,128)(2,1)S(1)} collective-permute-done((bf16[128,640]{1,0:T(8,128)(2,1)S(1)}, bf16[128,640]{1,0:T(8,128)(2,1)S(1)}, u32[]{:S(2)}, u32[]{:S(2)}) %collective-permute-start) | collective-permute-done | bytes 163872 | tf_op jit(solution)/shard_map/ppermute | solution.py:851
  29.9 1.6 %collective-permute-start.2 = (bf16[128,640]{1,0:T(8,128)(2,1)S(1)}, bf16[128,640]{1,0:T(8,128)(2,1)S(1)}, u32[]{:S(2)}, u32[]{:S(2)}) collective-permute-start(bf16[128,640]{1,0:T(8,128)(2,1)S(1)} %get-tuple-element.42.refs_0_.refs_4_), channel_id=1, source_target_pairs={{0,24},{4,28},{8,0},{12,4},{16,8},{20,12},{24,16},{28,20},{1,25},{... | collective-permute-start | bytes 491528 | tf_op jit(solution)/shard_map/ppermute | solution.py:851
  31.5 0.5 collective-permute-start.19
  32.0 4.2 %collective-permute-done.1.refs_2_ = bf16[128,640]{1,0:T(8,128)(2,1)S(1)} collective-permute-done((bf16[128,640]{1,0:T(8,128)(2,1)S(1)}, bf16[128,640]{1,0:T(8,128)(2,1)S(1)}, u32[]{:S(2)}, u32[]{:S(2)}) %collective-permute-start.1) | collective-permute-done | bytes 163872 | tf_op jit(solution)/shard_map/ppermute | solution.py:851
  36.2 1.7 %collective-permute-done.2.refs_3_ = bf16[128,640]{1,0:T(8,128)(2,1)S(1)} collective-permute-done((bf16[128,640]{1,0:T(8,128)(2,1)S(1)}, bf16[128,640]{1,0:T(8,128)(2,1)S(1)}, u32[]{:S(2)}, u32[]{:S(2)}) %collective-permute-start.2) | collective-permute-done | bytes 163872 | tf_op jit(solution)/shard_map/ppermute | solution.py:851
  38.0 0.6 collective-permute-start.12
  38.6 0.5 collective-permute-start.13
  39.1 5.3 %first_quarter.1 = (f32[4,96,1024]{2,1,0:T(8,128)S(1)}, bf16[2,384,192]{2,1,0:T(8,128)(2,1)S(1)}, bf16[2,192,384]{2,1,0:T(8,128)(2,1)S(1)}, f32[384,128]{1,0:T(8,128)S(1)}, bf16[2,1024,1024]{2,1,0:T(8,128)(2,1)S(1)}) custom-call(bf16[192,1024]{1,0:T(8,128)(2,1)S(1)} %get-tuple-element.49.xm, bf16[192,1024]{1,0:T(8,128)(2,1)S(1)} %collective-permute-done.16.xt, ...), custom_call_target="tpu_custom_call" | custom-call | flops 3000000000 | bytes 10000000 | tf_op jit(solution)/shard_map/first_quarter/pallas_call | solution.py:437
  44.5 0.9 collective-permute-done.12.m0
  45.9 4.7 %beside_quarters.1 = (f32[4,96,1024]{2,1,0:T(8,128)S(1)}, bf16[4,1024,1024]{2,1,0:T(8,128)(2,1)S(1)}, bf16[2048,1024]{1,0:T(8,128)(2,1)S(1)}) custom-call(bf16[192,1024]{1,0:T(8,128)(2,1)S(1)} %collective-permute-done.10.x_ref.xm, bf16[192,1024]{1,0:T(8,128)(2,1)S(1)} %collective-permute-done.18.xt, bf16[192,1024]{1,0:T(8,128)(2,1)S(1)} %collective-permute-done.11.y_ref.ym, ...), custom_call_target="tpu_custom_call" | custom-call | flops 3000000000 | bytes 10000000 | tf_op jit(solution)/shard_map/beside_quarters/pallas_call | solution.py:470
  50.6 3.5 %far_quarter.1 = (bf16[384,512]{1,0:T(8,128)(2,1)S(1)}, bf16[2048,1024]{1,0:T(8,128)(2,1)S(1)}, bf16[2048,1024]{1,0:T(8,128)(2,1)S(1)}) custom-call(bf16[96,1024]{1,0:T(8,128)(2,1)S(1)} %collective-permute-done.12.m0, bf16[96,1024]{1,0:T(8,128)(2,1)S(1)} %collective-permute-done.13.m1, bf16[96,1024]{1,0:T(8,128)(2,1)S(1)} %collective-permute-done.14.t0, ...), custom_call_target="tpu_custom_call" | custom-call | flops 3000000000 | bytes 10000000 | tf_op jit(solution)/shard_map/far_quarter/pallas_call | solution.py:516
  54.2 1.2 %down_quarter.6 = (f32[192,1024]{1,0:T(8,128)S(1)}, bf16[192,1024]{1,0:T(8,128)(2,1)S(1)}) custom-call(bf16[384,512]{1,0:T(8,128)(2,1)S(1)} %get-tuple-element.60.acts, bf16[2,192,384]{2,1,0:T(8,128)(2,1)S(1)} %get-tuple-element.61.back, bf16[2048,1024]{1,0:T(8,128)(2,1)S(1)} %get-tuple-element.68.wd), custom_call_target="tpu_custom_call" | custom-call | flops 1800000000 | bytes 6000000 | tf_op jit(solution)/shard_map/down_quarter/pallas_call | solution.py:559
  55.4 0.3 collective-permute-start.23
  55.7 1.2 %down_quarter.7 = (f32[192,1024]{1,0:T(8,128)S(1)}, bf16[192,1024]{1,0:T(8,128)(2,1)S(1)}) custom-call(bf16[384,512]{1,0:T(8,128)(2,1)S(1)} %get-tuple-element.60.acts, bf16[2,192,384]{2,1,0:T(8,128)(2,1)S(1)} %get-tuple-element.61.back, bf16[2048,1024]{1,0:T(8,128)(2,1)S(1)} %get-tuple-element.71.wd), custom_call_target="tpu_custom_call" | custom-call | flops 1800000000 | bytes 6000000 | tf_op jit(solution)/shard_map/down_quarter/pallas_call | solution.py:559
  56.9 0.3 collective-permute-start.24
  57.3 1.2 %down_quarter.5 = (f32[192,1024]{1,0:T(8,128)S(1)}, bf16[192,1024]{1,0:T(8,128)(2,1)S(1)}) custom-call(bf16[384,512]{1,0:T(8,128)(2,1)S(1)} %get-tuple-element.60.acts, bf16[2,192,384]{2,1,0:T(8,128)(2,1)S(1)} %get-tuple-element.61.back, bf16[2048,1024]{1,0:T(8,128)(2,1)S(1)} %get-tuple-element.65.wd), custom_call_target="tpu_custom_call" | custom-call | flops 1800000000 | bytes 6000000 | tf_op jit(solution)/shard_map/down_quarter/pallas_call | solution.py:559
  58.8 2.4 %attend.1 = (bf16[128,256]{1,0:T(8,128)(2,1)S(1)}, bf16[2048,1024]{1,0:T(8,128)(2,1)S(1)}) custom-call(bf16[512,384]{1,0:T(8,128)(2,1)S(1)} %get-tuple-element.41.stacked, bf16[512,640]{1,0:T(8,128)(2,1)S(1)} %stack_blocks.2.mine, bf16[512,640]{1,0:T(8,128)(2,1)S(1)} %collective-permute-done.3.twin, bf16[4,512,4096]{2,1,0:T(8,128)(2,1)} %wd.5), custom_call_target="tpu_custom_call" | custom-call | flops 5000000000 | bytes 4000000 | tf_op jit(solution)/shard_map/attend/pallas_call | solution.py:796
  61.3 1.6 %collective-permute-start.28 = (bf16[96,1024]{1,0:T(8,128)(2,1)S(1)}, bf16[96,1024]{1,0:T(8,128)(2,1)S(1)}, u32[]{:S(2)}, u32[]{:S(2)}) collective-permute-start(bf16[96,1024]{1,0:T(8,128)(2,1)S(1)} %sum_half.9), channel_id=1, source_target_pairs={{0,2},{1,3},{2,0},{3,1},{4,6},{5,7},{6,4},{7,5},{8,10},{9,11},{10,... | collective-permute-start | bytes 589832 | tf_op jit(solution)/shard_map/ppermute | solution.py:851
  62.9 1.2 %down_quarter.4 = (f32[192,1024]{1,0:T(8,128)S(1)}, bf16[192,1024]{1,0:T(8,128)(2,1)S(1)}) custom-call(bf16[384,512]{1,0:T(8,128)(2,1)S(1)} %get-tuple-element.60.acts, bf16[2,192,384]{2,1,0:T(8,128)(2,1)S(1)} %get-tuple-element.61.back, bf16[2048,1024]{1,0:T(8,128)(2,1)S(1)} %get-tuple-element.62.wd), custom_call_target="tpu_custom_call" | custom-call | flops 1800000000 | bytes 6000000 | tf_op jit(solution)/shard_map/down_quarter/pallas_call | solution.py:559
  64.3 0.7 collective-permute-start.25
  65.0 0.6 collective-permute-start.30
  65.6 3.6 %collective-permute-done.28.refs_0_ = bf16[96,1024]{1,0:T(8,128)(2,1)S(1)} collective-permute-done((bf16[96,1024]{1,0:T(8,128)(2,1)S(1)}, bf16[96,1024]{1,0:T(8,128)(2,1)S(1)}, u32[]{:S(2)}, u32[]{:S(2)}) %collective-permute-start.28) | collective-permute-done | bytes 196640 | tf_op jit(solution)/shard_map/ppermute | solution.py:851
  69.3 2.1 %collective-permute-start.22 = (bf16[96,1024]{1,0:T(8,128)(2,1)S(1)}, bf16[96,1024]{1,0:T(8,128)(2,1)S(1)}, u32[]{:S(2)}, u32[]{:S(2)}) collective-permute-start(bf16[96,1024]{1,0:T(8,128)(2,1)S(1)} %sum_half.6), channel_id=1, source_target_pairs={{0,1},{1,0},{2,3},{3,2},{4,5},{5,4},{6,7},{7,6},{8,9},{9,8},{10,11... | collective-permute-start | bytes 589832 | tf_op jit(solution)/shard_map/ppermute | solution.py:851
  71.4 0.7 collective-permute-done.25.refs_0_
  72.2 0.9 collective-permute-start.26
  73.1 0.5 collective-permute-start.4
  73.6 1.3 %collective-permute-start.5 = (bf16[128,256]{1,0:T(8,128)(2,1)S(1)}, bf16[128,256]{1,0:T(8,128)(2,1)S(1)}, u32[]{:S(2)}, u32[]{:S(2)}) collective-permute-start(bf16[128,256]{1,0:T(8,128)(2,1)S(1)} %get-tuple-element.43.refs_0_), channel_id=1, source_target_pairs={{0,2},{1,3},{2,0},{3,1},{4,6},{5,7},{6,4},{7,5},{8,10},{9,11},{10,... | collective-permute-start | bytes 196616 | tf_op jit(solution)/shard_map/ppermute | solution.py:851
  74.9 2.2 %collective-permute-done.29.x_part = bf16[96,1024]{1,0:T(8,128)(2,1)S(1)} collective-permute-done((bf16[96,1024]{1,0:T(8,128)(2,1)S(1)}, bf16[96,1024]{1,0:T(8,128)(2,1)S(1)}, u32[]{:S(2)}, u32[]{:S(2)}) %collective-permute-start.29) | collective-permute-done | bytes 196640 | tf_op jit(solution)/shard_map/ppermute | solution.py:851
  77.1 1.5 %collective-permute-start.6 = (bf16[128,256]{1,0:T(8,128)(2,1)S(1)}, bf16[128,256]{1,0:T(8,128)(2,1)S(1)}, u32[]{:S(2)}, u32[]{:S(2)}) collective-permute-start(bf16[128,256]{1,0:T(8,128)(2,1)S(1)} %get-tuple-element.43.refs_0_), channel_id=1, source_target_pairs={{0,3},{1,2},{2,1},{3,0},{4,7},{5,6},{6,5},{7,4},{8,11},{9,10},{10,... | collective-permute-start | bytes 196616 | tf_op jit(solution)/shard_map/ppermute | solution.py:851
  78.6 2.6 %collective-permute-done.22.x_part = bf16[96,1024]{1,0:T(8,128)(2,1)S(1)} collective-permute-done((bf16[96,1024]{1,0:T(8,128)(2,1)S(1)}, bf16[96,1024]{1,0:T(8,128)(2,1)S(1)}, u32[]{:S(2)}, u32[]{:S(2)}) %collective-permute-start.22) | collective-permute-done | bytes 196640 | tf_op jit(solution)/shard_map/ppermute | solution.py:851
  81.3 1.3 %collective-permute-start.31 = (bf16[48,1024]{1,0:T(8,128)(2,1)S(1)}, bf16[48,1024]{1,0:T(8,128)(2,1)S(1)}, u32[]{:S(2)}, u32[]{:S(2)}) collective-permute-start(bf16[48,1024]{1,0:T(8,128)(2,1)S(1)} %get-tuple-element.76), channel_id=1, source_target_pairs={{0,16},{4,20},{8,24},{12,28},{16,0},{20,4},{24,8},{28,12},{1,17},{... | collective-permute-start | bytes 294920 | tf_op jit(solution)/shard_map/ppermute | solution.py:851
  82.6 2.7 %collective-permute-start.32 = (bf16[48,1024]{1,0:T(8,128)(2,1)S(1)}, bf16[48,1024]{1,0:T(8,128)(2,1)S(1)}, u32[]{:S(2)}, u32[]{:S(2)}) collective-permute-start(bf16[48,1024]{1,0:T(8,128)(2,1)S(1)} %get-tuple-element.77), channel_id=1, source_target_pairs={{0,8},{4,12},{8,16},{12,20},{16,24},{20,28},{24,0},{28,4},{1,9},{5... | collective-permute-start | bytes 294920 | tf_op jit(solution)/shard_map/ppermute | solution.py:851
  85.3 1.2 %collective-permute-start.27 = (bf16[48,1024]{1,0:T(8,128)(2,1)S(1)}, bf16[48,1024]{1,0:T(8,128)(2,1)S(1)}, u32[]{:S(2)}, u32[]{:S(2)}) collective-permute-start(bf16[48,1024]{1,0:T(8,128)(2,1)S(1)} %get-tuple-element.75), channel_id=1, source_target_pairs={{0,24},{4,28},{8,0},{12,4},{16,8},{20,12},{24,16},{28,20},{1,25},{... | collective-permute-start | bytes 294920 | tf_op jit(solution)/shard_map/ppermute | solution.py:851
  86.6 1.2 %project.1 = bf16[128,1024]{1,0:T(8,128)(2,1)} custom-call(f32[1,1024]{1,0:T(1,128)S(1)} %bitcast.8, bf16[1024,1024]{1,0:T(8,128)(2,1)S(1)} %copy-done, bf16[128,256]{1,0:T(8,128)(2,1)S(1)} %get-tuple-element.43.refs_0_, bf16[128,256]{1,0:T(8,128)(2,1)S(1)} %collective-permute-done.4.refs_1_, bf16[128,256]{1,0:T(8,128)(2,1)S(1)} %collective-permute-done.5.refs_2_, ...), custom_call_target="tpu_custom_call" | custom-call | flops 1000000000 | bytes 3000000 | tf_op jit(solution)/shard_map/project/pallas_call | solution.py:829
  87.7 2.8 %collective-permute-done.31.refs_2_ = bf16[48,1024]{1,0:T(8,128)(2,1)S(1)} collective-permute-done((bf16[48,1024]{1,0:T(8,128)(2,1)S(1)}, bf16[48,1024]{1,0:T(8,128)(2,1)S(1)}, u32[]{:S(2)}, u32[]{:S(2)}) %collective-permute-start.31) | collective-permute-done | bytes 98336 | tf_op jit(solution)/shard_map/ppermute | solution.py:851
  90.5 0.7 collective-permute-done.27.refs_1_
  91.2 0.9 %place_rows.1 = bf16[128,1024]{1,0:T(8,128)(2,1)} custom-call(bf16[128,192]{1,0:T(8,128)(2,1)S(1)} %get-tuple-element.40.refs_12_.after.pick, bf16[48,1024]{1,0:T(8,128)(2,1)S(1)} %get-tuple-element.74.refs_0_, bf16[48,1024]{1,0:T(8,128)(2,1)S(1)} %collective-permute-done.27.refs_1_, bf16[48,1024]{1,0:T(8,128)(2,1)S(1)} %collective-permute-done.31.refs_2_, ...), custom_call_target="tpu_custom_call" | custom-call | flops 500000000 | bytes 1000000 | tf_op jit(solution)/shard_map/place_rows/pallas_call | solution.py:627
  (46 shorter events, 1.7 us)
Async XLA Ops:
  2.5 11.8 %collective-permute-start.7 = (bf16[48,1152]{1,0:T(8,128)(2,1)S(1)}, bf16[48,1152]{1,0:T(8,128)(2,1)S(1)}, u32[]{:S(2)}, u32[]{:S(2)}) collective-permute-start(bf16[48,1152]{1,0:T(8,128)(2,1)S(1)} %get-tuple-element.45), channel_id=1, source_target_pairs={{0,8},{4,12},{8,16},{12,20},{16,24},{20,28},{24,0},{28,4},{1,9},{5... | collective-permute-start | bytes 331784 | tf_op jit(solution)/shard_map/ppermute | solution.py:851
  5.6 9.9 %collective-permute-start.8 = (bf16[48,1152]{1,0:T(8,128)(2,1)S(1)}, bf16[48,1152]{1,0:T(8,128)(2,1)S(1)}, u32[]{:S(2)}, u32[]{:S(2)}) collective-permute-start(bf16[48,1152]{1,0:T(8,128)(2,1)S(1)} %get-tuple-element.46), channel_id=1, source_target_pairs={{0,16},{4,20},{8,24},{12,28},{16,0},{20,4},{24,8},{28,12},{1,17},{... | collective-permute-start | bytes 331784 | tf_op jit(solution)/shard_map/ppermute | solution.py:851
  8.2 7.3 %collective-permute-start.9 = (bf16[48,1152]{1,0:T(8,128)(2,1)S(1)}, bf16[48,1152]{1,0:T(8,128)(2,1)S(1)}, u32[]{:S(2)}, u32[]{:S(2)}) collective-permute-start(bf16[48,1152]{1,0:T(8,128)(2,1)S(1)} %get-tuple-element.47), channel_id=1, source_target_pairs={{0,24},{4,28},{8,0},{12,4},{16,8},{20,12},{24,16},{28,20},{1,25},{... | collective-permute-start | bytes 331784 | tf_op jit(solution)/shard_map/ppermute | solution.py:851
  15.5 23.0 %collective-permute-start.16 = (bf16[192,1024]{1,0:T(8,128)(2,1)S(1)}, bf16[192,1024]{1,0:T(8,128)(2,1)S(1)}, u32[]{:S(2)}, u32[]{:S(2)}) collective-permute-start(bf16[192,1024]{1,0:T(8,128)(2,1)S(1)} %get-tuple-element.49.xm), channel_id=1, source_target_pairs={{0,4},{4,0},{8,12},{12,8},{16,20},{20,16},{24,28},{28,24},{1,5},{5... | collective-permute-start | bytes 1179656 | tf_op jit(solution)/shard_map/ppermute | solution.py:851
  15.6 15.8 %collective-permute-start.10 = (bf16[192,1024]{1,0:T(8,128)(2,1)S(1)}, bf16[192,1024]{1,0:T(8,128)(2,1)S(1)}, u32[]{:S(2)}, u32[]{:S(2)}) collective-permute-start(bf16[192,1024]{1,0:T(8,128)(2,1)S(1)} %get-tuple-element.49.xm), channel_id=1, source_target_pairs={{0,1},{1,0},{2,3},{3,2},{4,5},{5,4},{6,7},{7,6},{8,9},{9,8},{10,11... | collective-permute-start | bytes 1179656 | tf_op jit(solution)/shard_map/ppermute | solution.py:851
  17.2 14.3 %collective-permute-start.11 = (bf16[192,1024]{1,0:T(8,128)(2,1)S(1)}, bf16[192,1024]{1,0:T(8,128)(2,1)S(1)}, u32[]{:S(2)}, u32[]{:S(2)}) collective-permute-start(bf16[192,1024]{1,0:T(8,128)(2,1)S(1)} %get-tuple-element.49.xm), channel_id=1, source_target_pairs={{0,2},{1,3},{2,0},{3,1},{4,6},{5,7},{6,4},{7,5},{8,10},{9,11},{10,... | collective-permute-start | bytes 1179656 | tf_op jit(solution)/shard_map/ppermute | solution.py:851
  20.9 9.1 %collective-permute-start = (bf16[128,640]{1,0:T(8,128)(2,1)S(1)}, bf16[128,640]{1,0:T(8,128)(2,1)S(1)}, u32[]{:S(2)}, u32[]{:S(2)}) collective-permute-start(bf16[128,640]{1,0:T(8,128)(2,1)S(1)} %get-tuple-element.42.refs_0_.refs_4_), channel_id=1, source_target_pairs={{0,8},{4,12},{8,16},{12,20},{16,24},{20,28},{24,0},{28,4},{1,9},{5... | collective-permute-start | bytes 491528 | tf_op jit(solution)/shard_map/ppermute | solution.py:851
  23.8 12.4 %collective-permute-start.1 = (bf16[128,640]{1,0:T(8,128)(2,1)S(1)}, bf16[128,640]{1,0:T(8,128)(2,1)S(1)}, u32[]{:S(2)}, u32[]{:S(2)}) collective-permute-start(bf16[128,640]{1,0:T(8,128)(2,1)S(1)} %get-tuple-element.42.refs_0_.refs_4_), channel_id=1, source_target_pairs={{0,16},{4,20},{8,24},{12,28},{16,0},{20,4},{24,8},{28,12},{1,17},{... | collective-permute-start | bytes 491528 | tf_op jit(solution)/shard_map/ppermute | solution.py:851
  29.9 7.9 %collective-permute-start.2 = (bf16[128,640]{1,0:T(8,128)(2,1)S(1)}, bf16[128,640]{1,0:T(8,128)(2,1)S(1)}, u32[]{:S(2)}, u32[]{:S(2)}) collective-permute-start(bf16[128,640]{1,0:T(8,128)(2,1)S(1)} %get-tuple-element.42.refs_0_.refs_4_), channel_id=1, source_target_pairs={{0,24},{4,28},{8,0},{12,4},{16,8},{20,12},{24,16},{28,20},{1,25},{... | collective-permute-start | bytes 491528 | tf_op jit(solution)/shard_map/ppermute | solution.py:851
  31.5 14.4 %collective-permute-start.18 = (bf16[192,1024]{1,0:T(8,128)(2,1)S(1)}, bf16[192,1024]{1,0:T(8,128)(2,1)S(1)}, u32[]{:S(2)}, u32[]{:S(2)}) collective-permute-start(bf16[192,1024]{1,0:T(8,128)(2,1)S(1)} %collective-permute-done.10.x_ref.xm), channel_id=1, source_target_pairs={{0,4},{4,0},{8,12},{12,8},{16,20},{20,16},{24,28},{28,24},{1,5},{5... | collective-permute-start | bytes 1179656 | tf_op jit(solution)/shard_map/ppermute | solution.py:851
  31.5 14.4 %collective-permute-start.19 = (bf16[192,1024]{1,0:T(8,128)(2,1)S(1)}, bf16[192,1024]{1,0:T(8,128)(2,1)S(1)}, u32[]{:S(2)}, u32[]{:S(2)}) collective-permute-start(bf16[192,1024]{1,0:T(8,128)(2,1)S(1)} %collective-permute-done.11.y_ref.ym), channel_id=1, source_target_pairs={{0,4},{4,0},{8,12},{12,8},{16,20},{20,16},{24,28},{28,24},{1,5},{5... | collective-permute-start | bytes 1179656 | tf_op jit(solution)/shard_map/ppermute | solution.py:851
  36.2 1.8 %collective-permute-start.17 = (bf16[192,128]{1,0:T(8,128)(2,1)S(1)}, bf16[192,128]{1,0:T(8,128)(2,1)S(1)}, u32[]{:S(2)}, u32[]{:S(2)}) collective-permute-start(bf16[192,128]{1,0:T(8,128)(2,1)S(1)} %get-tuple-element.52.mm), channel_id=1, source_target_pairs={{0,4},{4,0},{8,12},{12,8},{16,20},{20,16},{24,28},{28,24},{1,5},{5... | collective-permute-start | bytes 147464 | tf_op jit(solution)/shard_map/ppermute | solution.py:851
  37.9 20.9 %collective-permute-start.3 = (bf16[512,640]{1,0:T(8,128)(2,1)S(1)}, bf16[512,640]{1,0:T(8,128)(2,1)S(1)}, u32[]{:S(2)}, u32[]{:S(2)}) collective-permute-start(bf16[512,640]{1,0:T(8,128)(2,1)S(1)} %stack_blocks.2.mine), channel_id=1, source_target_pairs={{0,4},{4,0},{8,12},{12,8},{16,20},{20,16},{24,28},{28,24},{1,5},{5... | collective-permute-start | bytes 1966088 | tf_op jit(solution)/shard_map/ppermute | solution.py:851
  38.0 7.4 %collective-permute-start.12 = (bf16[96,1024]{1,0:T(8,128)(2,1)S(1)}, bf16[96,1024]{1,0:T(8,128)(2,1)S(1)}, u32[]{:S(2)}, u32[]{:S(2)}) collective-permute-start(bf16[96,1024]{1,0:T(8,128)(2,1)S(1)} %get-tuple-element.50), channel_id=1, source_target_pairs={{0,2},{1,3},{2,0},{3,1},{4,6},{5,7},{6,4},{7,5},{8,10},{9,11},{10,... | collective-permute-start | bytes 589832 | tf_op jit(solution)/shard_map/ppermute | solution.py:851
  38.6 7.0 %collective-permute-start.13 = (bf16[96,1024]{1,0:T(8,128)(2,1)S(1)}, bf16[96,1024]{1,0:T(8,128)(2,1)S(1)}, u32[]{:S(2)}, u32[]{:S(2)}) collective-permute-start(bf16[96,1024]{1,0:T(8,128)(2,1)S(1)} %get-tuple-element.51), channel_id=1, source_target_pairs={{0,1},{1,0},{2,3},{3,2},{4,5},{5,4},{6,7},{7,6},{8,9},{9,8},{10,11... | collective-permute-start | bytes 589832 | tf_op jit(solution)/shard_map/ppermute | solution.py:851
  45.4 5.2 %collective-permute-start.14 = (bf16[96,1024]{1,0:T(8,128)(2,1)S(1)}, bf16[96,1024]{1,0:T(8,128)(2,1)S(1)}, u32[]{:S(2)}, u32[]{:S(2)}) collective-permute-start(bf16[96,1024]{1,0:T(8,128)(2,1)S(1)} %collective-permute-done.12.m0), channel_id=1, source_target_pairs={{0,4},{4,0},{8,12},{12,8},{16,20},{20,16},{24,28},{28,24},{1,5},{5... | collective-permute-start | bytes 589832 | tf_op jit(solution)/shard_map/ppermute | solution.py:851
  45.6 5.0 %collective-permute-start.15 = (bf16[96,1024]{1,0:T(8,128)(2,1)S(1)}, bf16[96,1024]{1,0:T(8,128)(2,1)S(1)}, u32[]{:S(2)}, u32[]{:S(2)}) collective-permute-start(bf16[96,1024]{1,0:T(8,128)(2,1)S(1)} %collective-permute-done.13.m1), channel_id=1, source_target_pairs={{0,4},{4,0},{8,12},{12,8},{16,20},{20,16},{24,28},{28,24},{1,5},{5... | collective-permute-start | bytes 589832 | tf_op jit(solution)/shard_map/ppermute | solution.py:851
  55.4 9.6 %collective-permute-start.23 = (bf16[192,1024]{1,0:T(8,128)(2,1)S(1)}, bf16[192,1024]{1,0:T(8,128)(2,1)S(1)}, u32[]{:S(2)}, u32[]{:S(2)}) collective-permute-start(bf16[192,1024]{1,0:T(8,128)(2,1)S(1)} %get-tuple-element.70), channel_id=1, source_target_pairs={{0,4},{4,0},{8,12},{12,8},{16,20},{20,16},{24,28},{28,24},{1,5},{5... | collective-permute-start | bytes 1179656 | tf_op jit(solution)/shard_map/ppermute | solution.py:851
  56.9 4.3 %collective-permute-start.24 = (bf16[192,1024]{1,0:T(8,128)(2,1)S(1)}, bf16[192,1024]{1,0:T(8,128)(2,1)S(1)}, u32[]{:S(2)}, u32[]{:S(2)}) collective-permute-start(bf16[192,1024]{1,0:T(8,128)(2,1)S(1)} %get-tuple-element.73), channel_id=1, source_target_pairs={{0,4},{4,0},{8,12},{12,8},{16,20},{20,16},{24,28},{28,24},{1,5},{5... | collective-permute-start | bytes 1179656 | tf_op jit(solution)/shard_map/ppermute | solution.py:851
  58.5 7.1 %collective-permute-start.21 = (bf16[192,1024]{1,0:T(8,128)(2,1)S(1)}, bf16[192,1024]{1,0:T(8,128)(2,1)S(1)}, u32[]{:S(2)}, u32[]{:S(2)}) collective-permute-start(bf16[192,1024]{1,0:T(8,128)(2,1)S(1)} %get-tuple-element.67), channel_id=1, source_target_pairs={{0,4},{4,0},{8,12},{12,8},{16,20},{20,16},{24,28},{28,24},{1,5},{5... | collective-permute-start | bytes 1179656 | tf_op jit(solution)/shard_map/ppermute | solution.py:851
  61.3 7.8 %collective-permute-start.28 = (bf16[96,1024]{1,0:T(8,128)(2,1)S(1)}, bf16[96,1024]{1,0:T(8,128)(2,1)S(1)}, u32[]{:S(2)}, u32[]{:S(2)}) collective-permute-start(bf16[96,1024]{1,0:T(8,128)(2,1)S(1)} %sum_half.9), channel_id=1, source_target_pairs={{0,2},{1,3},{2,0},{3,1},{4,6},{5,7},{6,4},{7,5},{8,10},{9,11},{10,... | collective-permute-start | bytes 589832 | tf_op jit(solution)/shard_map/ppermute | solution.py:851
  64.1 8.9 %collective-permute-start.20 = (bf16[192,1024]{1,0:T(8,128)(2,1)S(1)}, bf16[192,1024]{1,0:T(8,128)(2,1)S(1)}, u32[]{:S(2)}, u32[]{:S(2)}) collective-permute-start(bf16[192,1024]{1,0:T(8,128)(2,1)S(1)} %get-tuple-element.64), channel_id=1, source_target_pairs={{0,4},{4,0},{8,12},{12,8},{16,20},{20,16},{24,28},{28,24},{1,5},{5... | collective-permute-start | bytes 1179656 | tf_op jit(solution)/shard_map/ppermute | solution.py:851
  64.3 7.8 %collective-permute-start.25 = (bf16[96,1024]{1,0:T(8,128)(2,1)S(1)}, bf16[96,1024]{1,0:T(8,128)(2,1)S(1)}, u32[]{:S(2)}, u32[]{:S(2)}) collective-permute-start(bf16[96,1024]{1,0:T(8,128)(2,1)S(1)} %sum_half.7), channel_id=1, source_target_pairs={{0,1},{1,0},{2,3},{3,2},{4,5},{5,4},{6,7},{7,6},{8,9},{9,8},{10,11... | collective-permute-start | bytes 589832 | tf_op jit(solution)/shard_map/ppermute | solution.py:851
  65.0 21.6 %copy-start = (bf16[1024,1024]{1,0:T(8,128)(2,1)S(1)}, bf16[1024,1024]{1,0:T(8,128)(2,1)}, u32[]{:S(2)}) copy-start(bf16[1024,1024]{1,0:T(8,128)(2,1)} %proj.1) | copy-start | bytes 6291460
  65.0 21.6 %copy-start.1 = (f32[1024]{0:T(1024)S(1)}, f32[1024]{0:T(1024)}, u32[]{:S(2)}) copy-start(f32[1024]{0:T(1024)} %param.29) | copy-start | bytes 12292
  65.0 8.6 %collective-permute-start.30 = (bf16[96,1024]{1,0:T(8,128)(2,1)S(1)}, bf16[96,1024]{1,0:T(8,128)(2,1)S(1)}, u32[]{:S(2)}, u32[]{:S(2)}) collective-permute-start(bf16[96,1024]{1,0:T(8,128)(2,1)S(1)} %sum_half.11), channel_id=1, source_target_pairs={{0,2},{1,3},{2,0},{3,1},{4,6},{5,7},{6,4},{7,5},{8,10},{9,11},{10,... | collective-permute-start | bytes 589832 | tf_op jit(solution)/shard_map/ppermute | solution.py:851
  69.2 7.8 %collective-permute-start.29 = (bf16[96,1024]{1,0:T(8,128)(2,1)S(1)}, bf16[96,1024]{1,0:T(8,128)(2,1)S(1)}, u32[]{:S(2)}, u32[]{:S(2)}) collective-permute-start(bf16[96,1024]{1,0:T(8,128)(2,1)S(1)} %sum_half.10), channel_id=1, source_target_pairs={{0,1},{1,0},{2,3},{3,2},{4,5},{5,4},{6,7},{7,6},{8,9},{9,8},{10,11... | collective-permute-start | bytes 589832 | tf_op jit(solution)/shard_map/ppermute | solution.py:851
  69.3 11.9 %collective-permute-start.22 = (bf16[96,1024]{1,0:T(8,128)(2,1)S(1)}, bf16[96,1024]{1,0:T(8,128)(2,1)S(1)}, u32[]{:S(2)}, u32[]{:S(2)}) collective-permute-start(bf16[96,1024]{1,0:T(8,128)(2,1)S(1)} %sum_half.6), channel_id=1, source_target_pairs={{0,1},{1,0},{2,3},{3,2},{4,5},{5,4},{6,7},{7,6},{8,9},{9,8},{10,11... | collective-permute-start | bytes 589832 | tf_op jit(solution)/shard_map/ppermute | solution.py:851
  72.2 10.4 %collective-permute-start.26 = (bf16[96,1024]{1,0:T(8,128)(2,1)S(1)}, bf16[96,1024]{1,0:T(8,128)(2,1)S(1)}, u32[]{:S(2)}, u32[]{:S(2)}) collective-permute-start(bf16[96,1024]{1,0:T(8,128)(2,1)S(1)} %sum_half.8), channel_id=1, source_target_pairs={{0,2},{1,3},{2,0},{3,1},{4,6},{5,7},{6,4},{7,5},{8,10},{9,11},{10,... | collective-permute-start | bytes 589832 | tf_op jit(solution)/shard_map/ppermute | solution.py:851
  73.1 12.2 %collective-permute-start.4 = (bf16[128,256]{1,0:T(8,128)(2,1)S(1)}, bf16[128,256]{1,0:T(8,128)(2,1)S(1)}, u32[]{:S(2)}, u32[]{:S(2)}) collective-permute-start(bf16[128,256]{1,0:T(8,128)(2,1)S(1)} %get-tuple-element.43.refs_0_), channel_id=1, source_target_pairs={{0,1},{1,0},{2,3},{3,2},{4,5},{5,4},{6,7},{7,6},{8,9},{9,8},{10,11... | collective-permute-start | bytes 196616 | tf_op jit(solution)/shard_map/ppermute | solution.py:851
  73.6 12.9 %collective-permute-start.5 = (bf16[128,256]{1,0:T(8,128)(2,1)S(1)}, bf16[128,256]{1,0:T(8,128)(2,1)S(1)}, u32[]{:S(2)}, u32[]{:S(2)}) collective-permute-start(bf16[128,256]{1,0:T(8,128)(2,1)S(1)} %get-tuple-element.43.refs_0_), channel_id=1, source_target_pairs={{0,2},{1,3},{2,0},{3,1},{4,6},{5,7},{6,4},{7,5},{8,10},{9,11},{10,... | collective-permute-start | bytes 196616 | tf_op jit(solution)/shard_map/ppermute | solution.py:851
  77.1 9.5 %collective-permute-start.6 = (bf16[128,256]{1,0:T(8,128)(2,1)S(1)}, bf16[128,256]{1,0:T(8,128)(2,1)S(1)}, u32[]{:S(2)}, u32[]{:S(2)}) collective-permute-start(bf16[128,256]{1,0:T(8,128)(2,1)S(1)} %get-tuple-element.43.refs_0_), channel_id=1, source_target_pairs={{0,3},{1,2},{2,1},{3,0},{4,7},{5,6},{6,5},{7,4},{8,11},{9,10},{10,... | collective-permute-start | bytes 196616 | tf_op jit(solution)/shard_map/ppermute | solution.py:851
  81.3 9.2 %collective-permute-start.31 = (bf16[48,1024]{1,0:T(8,128)(2,1)S(1)}, bf16[48,1024]{1,0:T(8,128)(2,1)S(1)}, u32[]{:S(2)}, u32[]{:S(2)}) collective-permute-start(bf16[48,1024]{1,0:T(8,128)(2,1)S(1)} %get-tuple-element.76), channel_id=1, source_target_pairs={{0,16},{4,20},{8,24},{12,28},{16,0},{20,4},{24,8},{28,12},{1,17},{... | collective-permute-start | bytes 294920 | tf_op jit(solution)/shard_map/ppermute | solution.py:851
  82.6 7.9 %collective-permute-start.32 = (bf16[48,1024]{1,0:T(8,128)(2,1)S(1)}, bf16[48,1024]{1,0:T(8,128)(2,1)S(1)}, u32[]{:S(2)}, u32[]{:S(2)}) collective-permute-start(bf16[48,1024]{1,0:T(8,128)(2,1)S(1)} %get-tuple-element.77), channel_id=1, source_target_pairs={{0,8},{4,12},{8,16},{12,20},{16,24},{20,28},{24,0},{28,4},{1,9},{5... | collective-permute-start | bytes 294920 | tf_op jit(solution)/shard_map/ppermute | solution.py:851
  85.3 5.8 %collective-permute-start.27 = (bf16[48,1024]{1,0:T(8,128)(2,1)S(1)}, bf16[48,1024]{1,0:T(8,128)(2,1)S(1)}, u32[]{:S(2)}, u32[]{:S(2)}) collective-permute-start(bf16[48,1024]{1,0:T(8,128)(2,1)S(1)} %get-tuple-element.75), channel_id=1, source_target_pairs={{0,24},{4,28},{8,0},{12,4},{16,8},{20,12},{24,16},{28,20},{1,25},{... | collective-permute-start | bytes 294920 | tf_op jit(solution)/shard_map/ppermute | solution.py:851

commit v2 on v1

--- a/solution.py
+++ b/solution.py
@@ -812,29 +812,29 @@
     )(stacked, mine, twin, in_hbm(w_down))
 
 
-def project_kernel(gain, proj, *refs):
-    parts, out = refs[:-1], refs[-1]
-    depth = parts[0].shape[1]
+def project_kernel(gain, proj, pair, far_pair, out):
+    count, depth = out.shape[0], pair.shape[1]
     total = jnp.zeros(out.shape, F32)
-    squares = jnp.zeros((out.shape[0], 1), F32)
-    for j, part in enumerate(parts):
+    squares = jnp.zeros((count, 1), F32)
+    for j in range(4):
         rows = pl.ds(pl.multiple_of((lax.axis_index("tp") ^ j) * depth, 128), depth)
-        value = part[...].astype(F32)
+        near = pl.ds((j & 1) * count, count)
+        value = (pair if j < 2 else far_pair)[near, :].astype(F32)
         squares += jnp.sum(value * value, axis=-1, keepdims=True)
         total += dot((value * gain[:, rows]).astype(BF16), proj[rows, :])
-    out[...] = (total * lax.rsqrt(squares / (depth * len(parts)) + EPS)).astype(BF16)
-
-
-def project(gain, proj, parts):
+    out[...] = (total * lax.rsqrt(squares / gain.shape[1] + EPS)).astype(BF16)
+
+
+def project(gain, proj, pair, far_pair):
     return pl.pallas_call(
         project_kernel,
-        out_shape=jax.ShapeDtypeStruct((parts[0].shape[0], proj.shape[1]), BF16),
-        in_specs=[WHOLE] * (2 + len(parts)),
+        out_shape=jax.ShapeDtypeStruct((pair.shape[0] // 2, proj.shape[1]), BF16),
+        in_specs=[WHOLE] * 4,
         out_specs=WHOLE,
         compiler_params=limits(16),
         cost_estimate=cost(1e9, 3e6),
         name="project",
-    )(gain[None], proj, *parts)
+    )(gain[None], proj, pair, far_pair)
 
 
 def twin_shards(
@@ -870,15 +870,15 @@
         key_gain, pick,
     )
     own, meta = stack_blocks(arrived, (width, META), near_x)
+    x_block, y_block = sideways(own, 1), sideways(own, 2)
     own_twin, meta_twin = across(own), across(meta)
-    x_block, y_block = sideways(own, 1), sideways(own, 2)
     kv_blocks = [kv] + [along(kv, k) for k in others]
     start, sel, back, weight, high_y = first_quarter(
         own, own_twin, meta, meta_twin, w_gate, w_up, chips, slots
     )
+    x_twin, y_twin = across(x_block), across(y_block)
     x_half, y_half = split_halves(x_block, y_block)
     far_first, far_second = sideways(x_half, 2), sideways(y_half, 1)
-    x_twin, y_twin = across(x_block), across(y_block)
     start, far_weights, down_d = beside_quarters(
         x_block, x_twin, y_block, y_twin, sel, start, near_x, low_y, high_y,
         w_gate, w_up, w_down,
@@ -905,12 +905,14 @@
     attn, down_own = attend(stacked, kv_mine, kv_twin, w_down, width, heads, chips)
     mine, twin = down_quarter(acts, back, down_own)
     twin = across(twin)
-    parts = [attn] + [sideways(attn, which) for which in range(1, tp)]
+    attn_x = sideways(attn, 1)
     second = join_half(1, mine, twin, x_second, y_second, slots)
     returned = [along(block, -k) for k, block in enumerate(second, middle)]
+    (pair,) = stack_blocks([attn, attn_x], (attn.shape[1],), kv)
+    far_pair = sideways(pair, 2)
     first = join_half(0, mine, twin, x_first, y_first, slots)
     returned = [along(first[k], -k) for k in range(1, middle)] + returned
-    mixed = project(out_gain, out_proj, parts)
+    mixed = project(out_gain, out_proj, pair, far_pair)
     expert_out = place_rows(pick, [first[0]] + returned)
     return (mixed, expert_out)
 

time: 92.3 us -> 94.1 us (1.020)
  waiting for transfers between devices: 25.4 us -> 28 us
    ppermute x33 -> x32, waiting for transfers between devices: 25.4 us -> 28 us  [send(): return lax.ppermute(values, axis, pairs)]
    ppermute x33 -> x32, starting transfers between devices: 33.6 us -> 32.8 us  [send(): return lax.ppermute(values, axis, pairs)]
  transfers between devices with their start and end apart: 33 -> 32, of which waited for: 12 -> 7; matrix products, arithmetic and copies ran while one was open for 0% -> 0% of each run, Pallas kernels for 32% -> 26%
where the time goes in v2:
time: 94.1 us; the launch traced here: 93.9 us
  starting transfers between devices  32.8 us (35%)
  Pallas kernels  32.3 us (34%)
  waiting for transfers between devices  28 us (30%)
    ppermute x32, starting transfers between devices, send(): return lax.ppermute(values, axis, pairs)  32.8 us
    ppermute x32, waiting for transfers between devices, send(): return lax.ppermute(values, axis, pairs)  28 us
    pallas_call x1, Pallas kernels, first_quarter(): pl.pallas_call(functools.partial(first_kernel, chips, slots, local), out_...  5.34 us
    pallas_call x4, Pallas kernels, down_quarter(): pl.pallas_call(functools.partial(down_kernel, wd.shape[0] // acts.shape[1...  4.92 us
    pallas_call x1, Pallas kernels, beside_quarters(): pl.pallas_call(beside_kernel, out_shape=[jax.ShapeDtypeStruct(start.shape...  4.73 us
    pallas_call x1, Pallas kernels, hold_up(): pl.pallas_call(hold_up_kernel, out_shape=[jax.ShapeDtypeStruct((local, wi...  4.7 us
    pallas_call x1, Pallas kernels, far_quarter(): pl.pallas_call(far_kernel, out_shape=[jax.ShapeDtypeStruct((sel.shape[1],...  3.52 us
    pallas_call x1, Pallas kernels, attend(): pl.pallas_call(functools.partial(attend_kernel, heads, chips), out_shape=...  2.45 us
  transfers between devices with their start and end apart: 32, of which 7 were waited for; matrix products, arithmetic and copies ran while one was open for 0% of the time, Pallas kernels for 26%

profile of v2, /device:TPU:0, one launch (start us, length us, event | category | flops | bytes accessed | tf_op | source)
XLA Modules:
  0.0 93.9 jit_solution(16778651515466749964)
XLA Ops:
  0.6 1.8 %dispatch.1 = (bf16[48,1152]{1,0:T(8,128)(2,1)S(1)}, bf16[48,1152]{1,0:T(8,128)(2,1)S(1)}, bf16[48,1152]{1,0:T(8,128)(2,1)S(1)}, bf16[48,1152]{1,0:T(8,128)(2,1)S(1)}, bf16[128,192]{1,0:T(8,128)(2,1)S(1)}) custom-call(bf16[128,4096]{1,0:T(8,128)(2,1)} %x_hbm.1, f32[1,4096]{1,0:T(1,128)} %bitcast.9, s32[2,128]{1,0:T(2,128)} %bitcast.12, f32[2,128]{1,0:T(2,128)} %bitcast.13), custom_call_target="tpu_custom_call" | custom-call | flops 2000000000 | bytes 4000000 | tf_op jit(solution)/shard_map/dispatch/pallas_call | solution.py:292
  2.5 3.1 %collective-permute-start.6 = (bf16[48,1152]{1,0:T(8,128)(2,1)S(1)}, bf16[48,1152]{1,0:T(8,128)(2,1)S(1)}, u32[]{:S(2)}, u32[]{:S(2)}) collective-permute-start(bf16[48,1152]{1,0:T(8,128)(2,1)S(1)} %get-tuple-element.45), channel_id=1, source_target_pairs={{0,8},{4,12},{8,16},{12,20},{16,24},{20,28},{24,0},{28,4},{1,9},{5... | collective-permute-start | bytes 331784 | tf_op jit(solution)/shard_map/ppermute | solution.py:851
  5.6 2.1 %attend_prep.1 = (bf16[128,640]{1,0:T(8,128)(2,1)S(1)}, bf16[512,384]{1,0:T(8,128)(2,1)S(1)}) custom-call(bf16[128,512]{1,0:T(8,128)(2,1)} %refs_0_.1, bf16[32,128]{1,0:T(8,128)(2,1)} %bitcast.10, f32[1,512]{1,0:T(1,128)} %bitcast.11, bf16[512,256]{1,0:T(8,128)(2,1)} %refs_3_.1, bf16[512,256]{1,0:T(8,128)(2,1)} %refs_4_.1, bf16[128,384]{1,0:T(8,128)(2,1)} %refs_5_.1, ...), custom_call_target="tpu_custom_call" | custom-call | flops 2000000000 | bytes 4000000 | tf_op jit(solution)/shard_map/attend_prep/pallas_call | solution.py:738
  7.7 1.6 %collective-permute-start = (bf16[128,640]{1,0:T(8,128)(2,1)S(1)}, bf16[128,640]{1,0:T(8,128)(2,1)S(1)}, u32[]{:S(2)}, u32[]{:S(2)}) collective-permute-start(bf16[128,640]{1,0:T(8,128)(2,1)S(1)} %get-tuple-element.42.refs_0_.refs_4_.refs_2_), channel_id=1, source_target_pairs={{0,8},{4,12},{8,16},{12,20},{16,24},{20,28},{24,0},{28,4},{1,9},{5... | collective-permute-start | bytes 491528 | tf_op jit(solution)/shard_map/ppermute | solution.py:851
  9.3 1.1 %collective-permute-start.1 = (bf16[128,640]{1,0:T(8,128)(2,1)S(1)}, bf16[128,640]{1,0:T(8,128)(2,1)S(1)}, u32[]{:S(2)}, u32[]{:S(2)}) collective-permute-start(bf16[128,640]{1,0:T(8,128)(2,1)S(1)} %get-tuple-element.42.refs_0_.refs_4_.refs_2_), channel_id=1, source_target_pairs={{0,16},{4,20},{8,24},{12,28},{16,0},{20,4},{24,8},{28,12},{1,17},{... | collective-permute-start | bytes 491528 | tf_op jit(solution)/shard_map/ppermute | solution.py:851
  10.4 2.8 %collective-permute-start.2 = (bf16[128,640]{1,0:T(8,128)(2,1)S(1)}, bf16[128,640]{1,0:T(8,128)(2,1)S(1)}, u32[]{:S(2)}, u32[]{:S(2)}) collective-permute-start(bf16[128,640]{1,0:T(8,128)(2,1)S(1)} %get-tuple-element.42.refs_0_.refs_4_.refs_2_), channel_id=1, source_target_pairs={{0,24},{4,28},{8,0},{12,4},{16,8},{20,12},{24,16},{28,20},{1,25},{... | collective-permute-start | bytes 491528 | tf_op jit(solution)/shard_map/ppermute | solution.py:851
  13.3 0.3 collective-permute-start.7
  13.6 1.2 %collective-permute-start.8 = (bf16[48,1152]{1,0:T(8,128)(2,1)S(1)}, bf16[48,1152]{1,0:T(8,128)(2,1)S(1)}, u32[]{:S(2)}, u32[]{:S(2)}) collective-permute-start(bf16[48,1152]{1,0:T(8,128)(2,1)S(1)} %get-tuple-element.47), channel_id=1, source_target_pairs={{0,24},{4,28},{8,0},{12,4},{16,8},{20,12},{24,16},{28,20},{1,25},{... | collective-permute-start | bytes 331784 | tf_op jit(solution)/shard_map/ppermute | solution.py:851
  14.8 4.7 %hold_up.1 = (bf16[4,1024,1024]{2,1,0:T(8,128)(2,1)S(1)}, bf16[2,1024,1024]{2,1,0:T(8,128)(2,1)S(1)}) custom-call(bf16[4,4096,512]{2,1,0:T(8,128)(2,1)} %wg.5, bf16[4,4096,512]{2,1,0:T(8,128)(2,1)} %wu.5, bf16[128,192]{1,0:T(8,128)(2,1)S(1)} %get-tuple-element.40.refs_12_.after.pick), custom_call_target="tpu_custom_call" | custom-call | flops 5000000000 | bytes 34000000 | tf_op jit(solution)/shard_map/hold_up/pallas_call | solution.py:351
  19.5 11.1 %collective-permute-done.7.refs_2_ = bf16[48,1152]{1,0:T(8,128)(2,1)S(1)} collective-permute-done((bf16[48,1152]{1,0:T(8,128)(2,1)S(1)}, bf16[48,1152]{1,0:T(8,128)(2,1)S(1)}, u32[]{:S(2)}, u32[]{:S(2)}) %collective-permute-start.7) | collective-permute-done | bytes 110624 | tf_op jit(solution)/shard_map/ppermute | solution.py:851
  30.6 1.5 %collective-permute-start.9 = (bf16[192,1024]{1,0:T(8,128)(2,1)S(1)}, bf16[192,1024]{1,0:T(8,128)(2,1)S(1)}, u32[]{:S(2)}, u32[]{:S(2)}) collective-permute-start(bf16[192,1024]{1,0:T(8,128)(2,1)S(1)} %get-tuple-element.49.xm), channel_id=1, source_target_pairs={{0,1},{1,0},{2,3},{3,2},{4,5},{5,4},{6,7},{7,6},{8,9},{9,8},{10,11... | collective-permute-start | bytes 1179656 | tf_op jit(solution)/shard_map/ppermute | solution.py:851
  32.2 1.5 %collective-permute-start.10 = (bf16[192,1024]{1,0:T(8,128)(2,1)S(1)}, bf16[192,1024]{1,0:T(8,128)(2,1)S(1)}, u32[]{:S(2)}, u32[]{:S(2)}) collective-permute-start(bf16[192,1024]{1,0:T(8,128)(2,1)S(1)} %get-tuple-element.49.xm), channel_id=1, source_target_pairs={{0,2},{1,3},{2,0},{3,1},{4,6},{5,7},{6,4},{7,5},{8,10},{9,11},{10,... | collective-permute-start | bytes 1179656 | tf_op jit(solution)/shard_map/ppermute | solution.py:851
  33.8 0.6 collective-permute-start.3
  34.4 7.2 %collective-permute-done.9.x_ref.xm = bf16[192,1024]{1,0:T(8,128)(2,1)S(1)} collective-permute-done((bf16[192,1024]{1,0:T(8,128)(2,1)S(1)}, bf16[192,1024]{1,0:T(8,128)(2,1)S(1)}, u32[]{:S(2)}, u32[]{:S(2)}) %collective-permute-start.9) | collective-permute-done | bytes 393248 | tf_op jit(solution)/shard_map/ppermute | solution.py:851
  41.7 1.2 %collective-permute-done.10.y_ref.ym = bf16[192,1024]{1,0:T(8,128)(2,1)S(1)} collective-permute-done((bf16[192,1024]{1,0:T(8,128)(2,1)S(1)}, bf16[192,1024]{1,0:T(8,128)(2,1)S(1)}, u32[]{:S(2)}, u32[]{:S(2)}) %collective-permute-start.10) | collective-permute-done | bytes 393248 | tf_op jit(solution)/shard_map/ppermute | solution.py:851
  42.9 1.6 %collective-permute-start.11 = (bf16[96,1024]{1,0:T(8,128)(2,1)S(1)}, bf16[96,1024]{1,0:T(8,128)(2,1)S(1)}, u32[]{:S(2)}, u32[]{:S(2)}) collective-permute-start(bf16[96,1024]{1,0:T(8,128)(2,1)S(1)} %get-tuple-element.50), channel_id=1, source_target_pairs={{0,2},{1,3},{2,0},{3,1},{4,6},{5,7},{6,4},{7,5},{8,10},{9,11},{10,... | collective-permute-start | bytes 589832 | tf_op jit(solution)/shard_map/ppermute | solution.py:851
  44.5 0.5 collective-permute-start.12
  45.0 0.5 collective-permute-start.18
  45.5 5.3 %first_quarter.1 = (f32[4,96,1024]{2,1,0:T(8,128)S(1)}, bf16[2,384,192]{2,1,0:T(8,128)(2,1)S(1)}, bf16[2,192,384]{2,1,0:T(8,128)(2,1)S(1)}, f32[384,128]{1,0:T(8,128)S(1)}, bf16[2,1024,1024]{2,1,0:T(8,128)(2,1)S(1)}) custom-call(bf16[192,1024]{1,0:T(8,128)(2,1)S(1)} %get-tuple-element.49.xm, bf16[192,1024]{1,0:T(8,128)(2,1)S(1)} %collective-permute-done.15.xt, ...), custom_call_target="tpu_custom_call" | custom-call | flops 3000000000 | bytes 10000000 | tf_op jit(solution)/shard_map/first_quarter/pallas_call | solution.py:437
  50.9 0.1 collective-permute-start.13
  51.0 0.4 collective-permute-start.14
  51.5 2.4 %attend.1 = (bf16[128,256]{1,0:T(8,128)(2,1)S(1)}, bf16[2048,1024]{1,0:T(8,128)(2,1)S(1)}) custom-call(bf16[512,384]{1,0:T(8,128)(2,1)S(1)} %get-tuple-element.41.stacked, bf16[512,640]{1,0:T(8,128)(2,1)S(1)} %stack_blocks.3.mine, bf16[512,640]{1,0:T(8,128)(2,1)S(1)} %collective-permute-done.3.twin, bf16[4,512,4096]{2,1,0:T(8,128)(2,1)} %wd.5), custom_call_target="tpu_custom_call" | custom-call | flops 5000000000 | bytes 4000000 | tf_op jit(solution)/shard_map/attend/pallas_call | solution.py:796
  53.9 4.7 %beside_quarters.1 = (f32[4,96,1024]{2,1,0:T(8,128)S(1)}, bf16[4,1024,1024]{2,1,0:T(8,128)(2,1)S(1)}, bf16[2048,1024]{1,0:T(8,128)(2,1)S(1)}) custom-call(bf16[192,1024]{1,0:T(8,128)(2,1)S(1)} %collective-permute-done.9.x_ref.xm, bf16[192,1024]{1,0:T(8,128)(2,1)S(1)} %collective-permute-done.17.xt, bf16[192,1024]{1,0:T(8,128)(2,1)S(1)} %collective-permute-done.10.y_ref.ym, ...), custom_call_target="tpu_custom_call" | custom-call | flops 3000000000 | bytes 10000000 | tf_op jit(solution)/shard_map/beside_quarters/pallas_call | solution.py:470
  58.7 3.5 %far_quarter.1 = (bf16[384,512]{1,0:T(8,128)(2,1)S(1)}, bf16[2048,1024]{1,0:T(8,128)(2,1)S(1)}, bf16[2048,1024]{1,0:T(8,128)(2,1)S(1)}) custom-call(bf16[96,1024]{1,0:T(8,128)(2,1)S(1)} %collective-permute-done.11.m0, bf16[96,1024]{1,0:T(8,128)(2,1)S(1)} %collective-permute-done.12.m1, bf16[96,1024]{1,0:T(8,128)(2,1)S(1)} %collective-permute-done.13.t0, ...), custom_call_target="tpu_custom_call" | custom-call | flops 3000000000 | bytes 10000000 | tf_op jit(solution)/shard_map/far_quarter/pallas_call | solution.py:516
  62.2 1.2 %down_quarter.7 = (f32[192,1024]{1,0:T(8,128)S(1)}, bf16[192,1024]{1,0:T(8,128)(2,1)S(1)}) custom-call(bf16[384,512]{1,0:T(8,128)(2,1)S(1)} %get-tuple-element.60.acts, bf16[2,192,384]{2,1,0:T(8,128)(2,1)S(1)} %get-tuple-element.61.back, bf16[2048,1024]{1,0:T(8,128)(2,1)S(1)} %get-tuple-element.71.wd), custom_call_target="tpu_custom_call" | custom-call | flops 1800000000 | bytes 6000000 | tf_op jit(solution)/shard_map/down_quarter/pallas_call | solution.py:559
  63.5 0.2 collective-permute-start.23
  63.6 1.2 %down_quarter.6 = (f32[192,1024]{1,0:T(8,128)S(1)}, bf16[192,1024]{1,0:T(8,128)(2,1)S(1)}) custom-call(bf16[384,512]{1,0:T(8,128)(2,1)S(1)} %get-tuple-element.60.acts, bf16[2,192,384]{2,1,0:T(8,128)(2,1)S(1)} %get-tuple-element.61.back, bf16[2048,1024]{1,0:T(8,128)(2,1)S(1)} %get-tuple-element.68.wd), custom_call_target="tpu_custom_call" | custom-call | flops 1800000000 | bytes 6000000 | tf_op jit(solution)/shard_map/down_quarter/pallas_call | solution.py:559
  64.8 0.5 collective-permute-start.22
  65.3 1.2 %down_quarter.5 = (f32[192,1024]{1,0:T(8,128)S(1)}, bf16[192,1024]{1,0:T(8,128)(2,1)S(1)}) custom-call(bf16[384,512]{1,0:T(8,128)(2,1)S(1)} %get-tuple-element.60.acts, bf16[2,192,384]{2,1,0:T(8,128)(2,1)S(1)} %get-tuple-element.61.back, bf16[2048,1024]{1,0:T(8,128)(2,1)S(1)} %get-tuple-element.65.wd), custom_call_target="tpu_custom_call" | custom-call | flops 1800000000 | bytes 6000000 | tf_op jit(solution)/shard_map/down_quarter/pallas_call | solution.py:559
  66.6 0.2 collective-permute-start.20
  66.7 1.2 %down_quarter.4 = (f32[192,1024]{1,0:T(8,128)S(1)}, bf16[192,1024]{1,0:T(8,128)(2,1)S(1)}) custom-call(bf16[384,512]{1,0:T(8,128)(2,1)S(1)} %get-tuple-element.60.acts, bf16[2,192,384]{2,1,0:T(8,128)(2,1)S(1)} %get-tuple-element.61.back, bf16[2048,1024]{1,0:T(8,128)(2,1)S(1)} %get-tuple-element.62.wd), custom_call_target="tpu_custom_call" | custom-call | flops 1800000000 | bytes 6000000 | tf_op jit(solution)/shard_map/down_quarter/pallas_call | solution.py:559
  67.9 0.5 collective-permute-start.19
  68.5 0.6 collective-permute-start.27
  69.1 1.5 %collective-permute-start.24 = (bf16[96,1024]{1,0:T(8,128)(2,1)S(1)}, bf16[96,1024]{1,0:T(8,128)(2,1)S(1)}, u32[]{:S(2)}, u32[]{:S(2)}) collective-permute-start(bf16[96,1024]{1,0:T(8,128)(2,1)S(1)} %sum_half.7), channel_id=1, source_target_pairs={{0,1},{1,0},{2,3},{3,2},{4,5},{5,4},{6,7},{7,6},{8,9},{9,8},{10,11... | collective-permute-start | bytes 589832 | tf_op jit(solution)/shard_map/ppermute | solution.py:851
  70.6 0.6 collective-permute-start.4
  71.2 1.6 %collective-permute-start.29 = (bf16[96,1024]{1,0:T(8,128)(2,1)S(1)}, bf16[96,1024]{1,0:T(8,128)(2,1)S(1)}, u32[]{:S(2)}, u32[]{:S(2)}) collective-permute-start(bf16[96,1024]{1,0:T(8,128)(2,1)S(1)} %sum_half.11), channel_id=1, source_target_pairs={{0,2},{1,3},{2,0},{3,1},{4,6},{5,7},{6,4},{7,5},{8,10},{9,11},{10,... | collective-permute-start | bytes 589832 | tf_op jit(solution)/shard_map/ppermute | solution.py:851
  72.8 3.5 %collective-permute-done.27.refs_0_ = bf16[96,1024]{1,0:T(8,128)(2,1)S(1)} collective-permute-done((bf16[96,1024]{1,0:T(8,128)(2,1)S(1)}, bf16[96,1024]{1,0:T(8,128)(2,1)S(1)}, u32[]{:S(2)}, u32[]{:S(2)}) %collective-permute-start.27) | collective-permute-done | bytes 196640 | tf_op jit(solution)/shard_map/ppermute | solution.py:851
  76.4 1.6 %collective-permute-start.28 = (bf16[96,1024]{1,0:T(8,128)(2,1)S(1)}, bf16[96,1024]{1,0:T(8,128)(2,1)S(1)}, u32[]{:S(2)}, u32[]{:S(2)}) collective-permute-start(bf16[96,1024]{1,0:T(8,128)(2,1)S(1)} %sum_half.10), channel_id=1, source_target_pairs={{0,1},{1,0},{2,3},{3,2},{4,5},{5,4},{6,7},{7,6},{8,9},{9,8},{10,11... | collective-permute-start | bytes 589832 | tf_op jit(solution)/shard_map/ppermute | solution.py:851
  78.0 0.6 collective-permute-start.21
  78.7 1.0 %collective-permute-start.25 = (bf16[96,1024]{1,0:T(8,128)(2,1)S(1)}, bf16[96,1024]{1,0:T(8,128)(2,1)S(1)}, u32[]{:S(2)}, u32[]{:S(2)}) collective-permute-start(bf16[96,1024]{1,0:T(8,128)(2,1)S(1)} %sum_half.8), channel_id=1, source_target_pairs={{0,2},{1,3},{2,0},{3,1},{4,6},{5,7},{6,4},{7,5},{8,10},{9,11},{10,... | collective-permute-start | bytes 589832 | tf_op jit(solution)/shard_map/ppermute | solution.py:851
  79.7 1.1 %collective-permute-start.5 = (bf16[256,256]{1,0:T(8,128)(2,1)S(1)}, bf16[256,256]{1,0:T(8,128)(2,1)S(1)}, u32[]{:S(2)}, u32[]{:S(2)}) collective-permute-start(bf16[256,256]{1,0:T(8,128)(2,1)S(1)} %stack_blocks.4.pair), channel_id=1, source_target_pairs={{0,2},{1,3},{2,0},{3,1},{4,6},{5,7},{6,4},{7,5},{8,10},{9,11},{10,... | collective-permute-start | bytes 393224 | tf_op jit(solution)/shard_map/ppermute | solution.py:851
  80.8 2.9 %collective-permute-done.28.x_part = bf16[96,1024]{1,0:T(8,128)(2,1)S(1)} collective-permute-done((bf16[96,1024]{1,0:T(8,128)(2,1)S(1)}, bf16[96,1024]{1,0:T(8,128)(2,1)S(1)}, u32[]{:S(2)}, u32[]{:S(2)}) %collective-permute-start.28) | collective-permute-done | bytes 196640 | tf_op jit(solution)/shard_map/ppermute | solution.py:851
  83.8 2.0 %collective-permute-start.30 = (bf16[48,1024]{1,0:T(8,128)(2,1)S(1)}, bf16[48,1024]{1,0:T(8,128)(2,1)S(1)}, u32[]{:S(2)}, u32[]{:S(2)}) collective-permute-start(bf16[48,1024]{1,0:T(8,128)(2,1)S(1)} %get-tuple-element.76), channel_id=1, source_target_pairs={{0,16},{4,20},{8,24},{12,28},{16,0},{20,4},{24,8},{28,12},{1,17},{... | collective-permute-start | bytes 294920 | tf_op jit(solution)/shard_map/ppermute | solution.py:851
  85.8 1.4 %collective-permute-start.31 = (bf16[48,1024]{1,0:T(8,128)(2,1)S(1)}, bf16[48,1024]{1,0:T(8,128)(2,1)S(1)}, u32[]{:S(2)}, u32[]{:S(2)}) collective-permute-start(bf16[48,1024]{1,0:T(8,128)(2,1)S(1)} %get-tuple-element.77), channel_id=1, source_target_pairs={{0,8},{4,12},{8,16},{12,20},{16,24},{20,28},{24,0},{28,4},{1,9},{5... | collective-permute-start | bytes 294920 | tf_op jit(solution)/shard_map/ppermute | solution.py:851
  87.3 2.5 %collective-permute-start.26 = (bf16[48,1024]{1,0:T(8,128)(2,1)S(1)}, bf16[48,1024]{1,0:T(8,128)(2,1)S(1)}, u32[]{:S(2)}, u32[]{:S(2)}) collective-permute-start(bf16[48,1024]{1,0:T(8,128)(2,1)S(1)} %get-tuple-element.75), channel_id=1, source_target_pairs={{0,24},{4,28},{8,0},{12,4},{16,8},{20,12},{24,16},{28,20},{1,25},{... | collective-permute-start | bytes 294920 | tf_op jit(solution)/shard_map/ppermute | solution.py:851
  89.8 1.2 %project.1 = bf16[128,1024]{1,0:T(8,128)(2,1)} custom-call(f32[1,1024]{1,0:T(1,128)S(1)} %bitcast.8, bf16[1024,1024]{1,0:T(8,128)(2,1)S(1)} %copy-done, bf16[256,256]{1,0:T(8,128)(2,1)S(1)} %stack_blocks.4.pair, bf16[256,256]{1,0:T(8,128)(2,1)S(1)} %collective-permute-done.5.far_pair), custom_call_target="tpu_custom_call" | custom-call | flops 1000000000 | bytes 3000000 | tf_op jit(solution)/shard_map/project/pallas_call | solution.py:829
  90.9 2.0 %collective-permute-done.31.refs_3_ = bf16[48,1024]{1,0:T(8,128)(2,1)S(1)} collective-permute-done((bf16[48,1024]{1,0:T(8,128)(2,1)S(1)}, bf16[48,1024]{1,0:T(8,128)(2,1)S(1)}, u32[]{:S(2)}, u32[]{:S(2)}) %collective-permute-start.31) | collective-permute-done | bytes 98336 | tf_op jit(solution)/shard_map/ppermute | solution.py:851
  93.0 0.9 place_rows.1
  (45 shorter events, 0.8 us)
Async XLA Ops:
  2.5 11.1 %collective-permute-start.6 = (bf16[48,1152]{1,0:T(8,128)(2,1)S(1)}, bf16[48,1152]{1,0:T(8,128)(2,1)S(1)}, u32[]{:S(2)}, u32[]{:S(2)}) collective-permute-start(bf16[48,1152]{1,0:T(8,128)(2,1)S(1)} %get-tuple-element.45), channel_id=1, source_target_pairs={{0,8},{4,12},{8,16},{12,20},{16,24},{20,28},{24,0},{28,4},{1,9},{5... | collective-permute-start | bytes 331784 | tf_op jit(solution)/shard_map/ppermute | solution.py:851
  7.7 26.0 %collective-permute-start = (bf16[128,640]{1,0:T(8,128)(2,1)S(1)}, bf16[128,640]{1,0:T(8,128)(2,1)S(1)}, u32[]{:S(2)}, u32[]{:S(2)}) collective-permute-start(bf16[128,640]{1,0:T(8,128)(2,1)S(1)} %get-tuple-element.42.refs_0_.refs_4_.refs_2_), channel_id=1, source_target_pairs={{0,8},{4,12},{8,16},{12,20},{16,24},{20,28},{24,0},{28,4},{1,9},{5... | collective-permute-start | bytes 491528 | tf_op jit(solution)/shard_map/ppermute | solution.py:851
  9.3 24.4 %collective-permute-start.1 = (bf16[128,640]{1,0:T(8,128)(2,1)S(1)}, bf16[128,640]{1,0:T(8,128)(2,1)S(1)}, u32[]{:S(2)}, u32[]{:S(2)}) collective-permute-start(bf16[128,640]{1,0:T(8,128)(2,1)S(1)} %get-tuple-element.42.refs_0_.refs_4_.refs_2_), channel_id=1, source_target_pairs={{0,16},{4,20},{8,24},{12,28},{16,0},{20,4},{24,8},{28,12},{1,17},{... | collective-permute-start | bytes 491528 | tf_op jit(solution)/shard_map/ppermute | solution.py:851
  10.4 23.3 %collective-permute-start.2 = (bf16[128,640]{1,0:T(8,128)(2,1)S(1)}, bf16[128,640]{1,0:T(8,128)(2,1)S(1)}, u32[]{:S(2)}, u32[]{:S(2)}) collective-permute-start(bf16[128,640]{1,0:T(8,128)(2,1)S(1)} %get-tuple-element.42.refs_0_.refs_4_.refs_2_), channel_id=1, source_target_pairs={{0,24},{4,28},{8,0},{12,4},{16,8},{20,12},{24,16},{28,20},{1,25},{... | collective-permute-start | bytes 491528 | tf_op jit(solution)/shard_map/ppermute | solution.py:851
  13.3 17.3 %collective-permute-start.7 = (bf16[48,1152]{1,0:T(8,128)(2,1)S(1)}, bf16[48,1152]{1,0:T(8,128)(2,1)S(1)}, u32[]{:S(2)}, u32[]{:S(2)}) collective-permute-start(bf16[48,1152]{1,0:T(8,128)(2,1)S(1)} %get-tuple-element.46), channel_id=1, source_target_pairs={{0,16},{4,20},{8,24},{12,28},{16,0},{20,4},{24,8},{28,12},{1,17},{... | collective-permute-start | bytes 331784 | tf_op jit(solution)/shard_map/ppermute | solution.py:851
  13.6 17.0 %collective-permute-start.8 = (bf16[48,1152]{1,0:T(8,128)(2,1)S(1)}, bf16[48,1152]{1,0:T(8,128)(2,1)S(1)}, u32[]{:S(2)}, u32[]{:S(2)}) collective-permute-start(bf16[48,1152]{1,0:T(8,128)(2,1)S(1)} %get-tuple-element.47), channel_id=1, source_target_pairs={{0,24},{4,28},{8,0},{12,4},{16,8},{20,12},{24,16},{28,20},{1,25},{... | collective-permute-start | bytes 331784 | tf_op jit(solution)/shard_map/ppermute | solution.py:851
  30.6 11.0 %collective-permute-start.9 = (bf16[192,1024]{1,0:T(8,128)(2,1)S(1)}, bf16[192,1024]{1,0:T(8,128)(2,1)S(1)}, u32[]{:S(2)}, u32[]{:S(2)}) collective-permute-start(bf16[192,1024]{1,0:T(8,128)(2,1)S(1)} %get-tuple-element.49.xm), channel_id=1, source_target_pairs={{0,1},{1,0},{2,3},{3,2},{4,5},{5,4},{6,7},{7,6},{8,9},{9,8},{10,11... | collective-permute-start | bytes 1179656 | tf_op jit(solution)/shard_map/ppermute | solution.py:851
  32.2 10.7 %collective-permute-start.10 = (bf16[192,1024]{1,0:T(8,128)(2,1)S(1)}, bf16[192,1024]{1,0:T(8,128)(2,1)S(1)}, u32[]{:S(2)}, u32[]{:S(2)}) collective-permute-start(bf16[192,1024]{1,0:T(8,128)(2,1)S(1)} %get-tuple-element.49.xm), channel_id=1, source_target_pairs={{0,2},{1,3},{2,0},{3,1},{4,6},{5,7},{6,4},{7,5},{8,10},{9,11},{10,... | collective-permute-start | bytes 1179656 | tf_op jit(solution)/shard_map/ppermute | solution.py:851
  33.7 11.3 %collective-permute-start.15 = (bf16[192,1024]{1,0:T(8,128)(2,1)S(1)}, bf16[192,1024]{1,0:T(8,128)(2,1)S(1)}, u32[]{:S(2)}, u32[]{:S(2)}) collective-permute-start(bf16[192,1024]{1,0:T(8,128)(2,1)S(1)} %get-tuple-element.49.xm), channel_id=1, source_target_pairs={{0,4},{4,0},{8,12},{12,8},{16,20},{20,16},{24,28},{28,24},{1,5},{5... | collective-permute-start | bytes 1179656 | tf_op jit(solution)/shard_map/ppermute | solution.py:851
  33.8 17.7 %collective-permute-start.3 = (bf16[512,640]{1,0:T(8,128)(2,1)S(1)}, bf16[512,640]{1,0:T(8,128)(2,1)S(1)}, u32[]{:S(2)}, u32[]{:S(2)}) collective-permute-start(bf16[512,640]{1,0:T(8,128)(2,1)S(1)} %stack_blocks.3.mine), channel_id=1, source_target_pairs={{0,4},{4,0},{8,12},{12,8},{16,20},{20,16},{24,28},{28,24},{1,5},{5... | collective-permute-start | bytes 1966088 | tf_op jit(solution)/shard_map/ppermute | solution.py:851
  34.3 10.7 %collective-permute-start.16 = (bf16[192,128]{1,0:T(8,128)(2,1)S(1)}, bf16[192,128]{1,0:T(8,128)(2,1)S(1)}, u32[]{:S(2)}, u32[]{:S(2)}) collective-permute-start(bf16[192,128]{1,0:T(8,128)(2,1)S(1)} %get-tuple-element.52.mm), channel_id=1, source_target_pairs={{0,4},{4,0},{8,12},{12,8},{16,20},{20,16},{24,28},{28,24},{1,5},{5... | collective-permute-start | bytes 147464 | tf_op jit(solution)/shard_map/ppermute | solution.py:851
  42.9 8.0 %collective-permute-start.11 = (bf16[96,1024]{1,0:T(8,128)(2,1)S(1)}, bf16[96,1024]{1,0:T(8,128)(2,1)S(1)}, u32[]{:S(2)}, u32[]{:S(2)}) collective-permute-start(bf16[96,1024]{1,0:T(8,128)(2,1)S(1)} %get-tuple-element.50), channel_id=1, source_target_pairs={{0,2},{1,3},{2,0},{3,1},{4,6},{5,7},{6,4},{7,5},{8,10},{9,11},{10,... | collective-permute-start | bytes 589832 | tf_op jit(solution)/shard_map/ppermute | solution.py:851
  44.5 6.5 %collective-permute-start.12 = (bf16[96,1024]{1,0:T(8,128)(2,1)S(1)}, bf16[96,1024]{1,0:T(8,128)(2,1)S(1)}, u32[]{:S(2)}, u32[]{:S(2)}) collective-permute-start(bf16[96,1024]{1,0:T(8,128)(2,1)S(1)} %get-tuple-element.51), channel_id=1, source_target_pairs={{0,1},{1,0},{2,3},{3,2},{4,5},{5,4},{6,7},{7,6},{8,9},{9,8},{10,11... | collective-permute-start | bytes 589832 | tf_op jit(solution)/shard_map/ppermute | solution.py:851
  45.0 8.9 %collective-permute-start.17 = (bf16[192,1024]{1,0:T(8,128)(2,1)S(1)}, bf16[192,1024]{1,0:T(8,128)(2,1)S(1)}, u32[]{:S(2)}, u32[]{:S(2)}) collective-permute-start(bf16[192,1024]{1,0:T(8,128)(2,1)S(1)} %collective-permute-done.9.x_ref.xm), channel_id=1, source_target_pairs={{0,4},{4,0},{8,12},{12,8},{16,20},{20,16},{24,28},{28,24},{1,5},{5... | collective-permute-start | bytes 1179656 | tf_op jit(solution)/shard_map/ppermute | solution.py:851
  45.0 8.9 %collective-permute-start.18 = (bf16[192,1024]{1,0:T(8,128)(2,1)S(1)}, bf16[192,1024]{1,0:T(8,128)(2,1)S(1)}, u32[]{:S(2)}, u32[]{:S(2)}) collective-permute-start(bf16[192,1024]{1,0:T(8,128)(2,1)S(1)} %collective-permute-done.10.y_ref.ym), channel_id=1, source_target_pairs={{0,4},{4,0},{8,12},{12,8},{16,20},{20,16},{24,28},{28,24},{1,5},{5... | collective-permute-start | bytes 1179656 | tf_op jit(solution)/shard_map/ppermute | solution.py:851
  50.9 7.8 %collective-permute-start.13 = (bf16[96,1024]{1,0:T(8,128)(2,1)S(1)}, bf16[96,1024]{1,0:T(8,128)(2,1)S(1)}, u32[]{:S(2)}, u32[]{:S(2)}) collective-permute-start(bf16[96,1024]{1,0:T(8,128)(2,1)S(1)} %collective-permute-done.11.m0), channel_id=1, source_target_pairs={{0,4},{4,0},{8,12},{12,8},{16,20},{20,16},{24,28},{28,24},{1,5},{5... | collective-permute-start | bytes 589832 | tf_op jit(solution)/shard_map/ppermute | solution.py:851
  51.0 7.7 %collective-permute-start.14 = (bf16[96,1024]{1,0:T(8,128)(2,1)S(1)}, bf16[96,1024]{1,0:T(8,128)(2,1)S(1)}, u32[]{:S(2)}, u32[]{:S(2)}) collective-permute-start(bf16[96,1024]{1,0:T(8,128)(2,1)S(1)} %collective-permute-done.12.m1), channel_id=1, source_target_pairs={{0,4},{4,0},{8,12},{12,8},{16,20},{20,16},{24,28},{28,24},{1,5},{5... | collective-permute-start | bytes 589832 | tf_op jit(solution)/shard_map/ppermute | solution.py:851
  63.5 5.0 %collective-permute-start.23 = (bf16[192,1024]{1,0:T(8,128)(2,1)S(1)}, bf16[192,1024]{1,0:T(8,128)(2,1)S(1)}, u32[]{:S(2)}, u32[]{:S(2)}) collective-permute-start(bf16[192,1024]{1,0:T(8,128)(2,1)S(1)} %get-tuple-element.73), channel_id=1, source_target_pairs={{0,4},{4,0},{8,12},{12,8},{16,20},{20,16},{24,28},{28,24},{1,5},{5... | collective-permute-start | bytes 1179656 | tf_op jit(solution)/shard_map/ppermute | solution.py:851
  64.8 5.8 %collective-permute-start.22 = (bf16[192,1024]{1,0:T(8,128)(2,1)S(1)}, bf16[192,1024]{1,0:T(8,128)(2,1)S(1)}, u32[]{:S(2)}, u32[]{:S(2)}) collective-permute-start(bf16[192,1024]{1,0:T(8,128)(2,1)S(1)} %get-tuple-element.70), channel_id=1, source_target_pairs={{0,4},{4,0},{8,12},{12,8},{16,20},{20,16},{24,28},{28,24},{1,5},{5... | collective-permute-start | bytes 1179656 | tf_op jit(solution)/shard_map/ppermute | solution.py:851
  66.6 4.7 %collective-permute-start.20 = (bf16[192,1024]{1,0:T(8,128)(2,1)S(1)}, bf16[192,1024]{1,0:T(8,128)(2,1)S(1)}, u32[]{:S(2)}, u32[]{:S(2)}) collective-permute-start(bf16[192,1024]{1,0:T(8,128)(2,1)S(1)} %get-tuple-element.67), channel_id=1, source_target_pairs={{0,4},{4,0},{8,12},{12,8},{16,20},{20,16},{24,28},{28,24},{1,5},{5... | collective-permute-start | bytes 1179656 | tf_op jit(solution)/shard_map/ppermute | solution.py:851
  67.9 11.8 %collective-permute-start.19 = (bf16[192,1024]{1,0:T(8,128)(2,1)S(1)}, bf16[192,1024]{1,0:T(8,128)(2,1)S(1)}, u32[]{:S(2)}, u32[]{:S(2)}) collective-permute-start(bf16[192,1024]{1,0:T(8,128)(2,1)S(1)} %get-tuple-element.64), channel_id=1, source_target_pairs={{0,4},{4,0},{8,12},{12,8},{16,20},{20,16},{24,28},{28,24},{1,5},{5... | collective-permute-start | bytes 1179656 | tf_op jit(solution)/shard_map/ppermute | solution.py:851
  68.5 7.8 %collective-permute-start.27 = (bf16[96,1024]{1,0:T(8,128)(2,1)S(1)}, bf16[96,1024]{1,0:T(8,128)(2,1)S(1)}, u32[]{:S(2)}, u32[]{:S(2)}) collective-permute-start(bf16[96,1024]{1,0:T(8,128)(2,1)S(1)} %sum_half.9), channel_id=1, source_target_pairs={{0,2},{1,3},{2,0},{3,1},{4,6},{5,7},{6,4},{7,5},{8,10},{9,11},{10,... | collective-permute-start | bytes 589832 | tf_op jit(solution)/shard_map/ppermute | solution.py:851
  69.1 8.9 %collective-permute-start.24 = (bf16[96,1024]{1,0:T(8,128)(2,1)S(1)}, bf16[96,1024]{1,0:T(8,128)(2,1)S(1)}, u32[]{:S(2)}, u32[]{:S(2)}) collective-permute-start(bf16[96,1024]{1,0:T(8,128)(2,1)S(1)} %sum_half.7), channel_id=1, source_target_pairs={{0,1},{1,0},{2,3},{3,2},{4,5},{5,4},{6,7},{7,6},{8,9},{9,8},{10,11... | collective-permute-start | bytes 589832 | tf_op jit(solution)/shard_map/ppermute | solution.py:851
  70.6 8.0 %collective-permute-start.4 = (bf16[128,256]{1,0:T(8,128)(2,1)S(1)}, bf16[128,256]{1,0:T(8,128)(2,1)S(1)}, u32[]{:S(2)}, u32[]{:S(2)}) collective-permute-start(bf16[128,256]{1,0:T(8,128)(2,1)S(1)} %get-tuple-element.43.refs_0_), channel_id=1, source_target_pairs={{0,1},{1,0},{2,3},{3,2},{4,5},{5,4},{6,7},{7,6},{8,9},{9,8},{10,11... | collective-permute-start | bytes 196616 | tf_op jit(solution)/shard_map/ppermute | solution.py:851
  71.2 9.6 %collective-permute-start.29 = (bf16[96,1024]{1,0:T(8,128)(2,1)S(1)}, bf16[96,1024]{1,0:T(8,128)(2,1)S(1)}, u32[]{:S(2)}, u32[]{:S(2)}) collective-permute-start(bf16[96,1024]{1,0:T(8,128)(2,1)S(1)} %sum_half.11), channel_id=1, source_target_pairs={{0,2},{1,3},{2,0},{3,1},{4,6},{5,7},{6,4},{7,5},{8,10},{9,11},{10,... | collective-permute-start | bytes 589832 | tf_op jit(solution)/shard_map/ppermute | solution.py:851
  76.3 13.4 %copy-start = (bf16[1024,1024]{1,0:T(8,128)(2,1)S(1)}, bf16[1024,1024]{1,0:T(8,128)(2,1)}, u32[]{:S(2)}) copy-start(bf16[1024,1024]{1,0:T(8,128)(2,1)} %proj.1) | copy-start | bytes 6291460
  76.3 13.4 %copy-start.1 = (f32[1024]{0:T(1024)S(1)}, f32[1024]{0:T(1024)}, u32[]{:S(2)}) copy-start(f32[1024]{0:T(1024)} %param.29) | copy-start | bytes 12292
  76.4 7.3 %collective-permute-start.28 = (bf16[96,1024]{1,0:T(8,128)(2,1)S(1)}, bf16[96,1024]{1,0:T(8,128)(2,1)S(1)}, u32[]{:S(2)}, u32[]{:S(2)}) collective-permute-start(bf16[96,1024]{1,0:T(8,128)(2,1)S(1)} %sum_half.10), channel_id=1, source_target_pairs={{0,1},{1,0},{2,3},{3,2},{4,5},{5,4},{6,7},{7,6},{8,9},{9,8},{10,11... | collective-permute-start | bytes 589832 | tf_op jit(solution)/shard_map/ppermute | solution.py:851
  78.0 9.2 %collective-permute-start.21 = (bf16[96,1024]{1,0:T(8,128)(2,1)S(1)}, bf16[96,1024]{1,0:T(8,128)(2,1)S(1)}, u32[]{:S(2)}, u32[]{:S(2)}) collective-permute-start(bf16[96,1024]{1,0:T(8,128)(2,1)S(1)} %sum_half.6), channel_id=1, source_target_pairs={{0,1},{1,0},{2,3},{3,2},{4,5},{5,4},{6,7},{7,6},{8,9},{9,8},{10,11... | collective-permute-start | bytes 589832 | tf_op jit(solution)/shard_map/ppermute | solution.py:851
  78.7 8.5 %collective-permute-start.25 = (bf16[96,1024]{1,0:T(8,128)(2,1)S(1)}, bf16[96,1024]{1,0:T(8,128)(2,1)S(1)}, u32[]{:S(2)}, u32[]{:S(2)}) collective-permute-start(bf16[96,1024]{1,0:T(8,128)(2,1)S(1)} %sum_half.8), channel_id=1, source_target_pairs={{0,2},{1,3},{2,0},{3,1},{4,6},{5,7},{6,4},{7,5},{8,10},{9,11},{10,... | collective-permute-start | bytes 589832 | tf_op jit(solution)/shard_map/ppermute | solution.py:851
  79.7 10.0 %collective-permute-start.5 = (bf16[256,256]{1,0:T(8,128)(2,1)S(1)}, bf16[256,256]{1,0:T(8,128)(2,1)S(1)}, u32[]{:S(2)}, u32[]{:S(2)}) collective-permute-start(bf16[256,256]{1,0:T(8,128)(2,1)S(1)} %stack_blocks.4.pair), channel_id=1, source_target_pairs={{0,2},{1,3},{2,0},{3,1},{4,6},{5,7},{6,4},{7,5},{8,10},{9,11},{10,... | collective-permute-start | bytes 393224 | tf_op jit(solution)/shard_map/ppermute | solution.py:851
  83.8 7.1 %collective-permute-start.30 = (bf16[48,1024]{1,0:T(8,128)(2,1)S(1)}, bf16[48,1024]{1,0:T(8,128)(2,1)S(1)}, u32[]{:S(2)}, u32[]{:S(2)}) collective-permute-start(bf16[48,1024]{1,0:T(8,128)(2,1)S(1)} %get-tuple-element.76), channel_id=1, source_target_pairs={{0,16},{4,20},{8,24},{12,28},{16,0},{20,4},{24,8},{28,12},{1,17},{... | collective-permute-start | bytes 294920 | tf_op jit(solution)/shard_map/ppermute | solution.py:851
  85.8 7.1 %collective-permute-start.31 = (bf16[48,1024]{1,0:T(8,128)(2,1)S(1)}, bf16[48,1024]{1,0:T(8,128)(2,1)S(1)}, u32[]{:S(2)}, u32[]{:S(2)}) collective-permute-start(bf16[48,1024]{1,0:T(8,128)(2,1)S(1)} %get-tuple-element.77), channel_id=1, source_target_pairs={{0,8},{4,12},{8,16},{12,20},{16,24},{20,28},{24,0},{28,4},{1,9},{5... | collective-permute-start | bytes 294920 | tf_op jit(solution)/shard_map/ppermute | solution.py:851
  87.3 5.7 %collective-permute-start.26 = (bf16[48,1024]{1,0:T(8,128)(2,1)S(1)}, bf16[48,1024]{1,0:T(8,128)(2,1)S(1)}, u32[]{:S(2)}, u32[]{:S(2)}) collective-permute-start(bf16[48,1024]{1,0:T(8,128)(2,1)S(1)} %get-tuple-element.75), channel_id=1, source_target_pairs={{0,24},{4,28},{8,0},{12,4},{16,8},{20,12},{24,16},{28,20},{1,25},{... | collective-permute-start | bytes 294920 | tf_op jit(solution)/shard_map/ppermute | solution.py:851
